TPU v7x, 256 devices: a 4x2x16 block of a 4x16x16 slice. The times are simulated.
256 devices in a mesh: grp: 2 (over y), sp: 32 (over z, core), tp: 4 (over x).
Axes of the slice: x: 4, y: 2, z: 16, core: 2. Of those that a mesh axis runs over, the one named last changes fastest.
The devices are a block of a 4x16x16 slice.
Arguments:
- residual_in: bfloat16 [20480, 2048], P(('grp', 'sp', 'tp')), parts along dimension 0, may hold values from -6 to 6
- narrow_query_rows: bfloat16 [20480, 1024], P(('grp', 'sp'), 'tp'), parts along dimension 0, may hold values from -5 to 5
- wide_query_rows: bfloat16 [20480, 1024], P(('grp', 'sp'), 'tp'), parts along dimension 0, may hold values from -5 to 5
- narrow_key_value: bfloat16 [20480, 4, 128], P(('grp', 'sp'), 'tp'), parts along dimension 0, may hold values from -120 to 120
- wide_key_value: bfloat16 [20480, 4, 256], P(('grp', 'sp'), 'tp'), parts along dimension 0, may hold values from -120 to 120
- narrow_norm_gains: float32 [2, 64], replicated, may hold values from 0.1 to 10
- wide_norm_gains: float32 [2, 128], replicated, may hold values from 0.1 to 10
- out_narrow: bfloat16 [1024, 2048], P('tp'), may hold values from -0.1875 to 0.1875
- out_wide: bfloat16 [1024, 2048], P('tp'), may hold values from -0.1875 to 0.1875
- mixer_gain: float32 [2048], replicated, may hold values from 0.1 to 1.9
- mixer_gate: bfloat16 [2048, 5632], P('sp', 'tp'), may hold values from -0.125 to 0.125
- mixer_up: bfloat16 [2048, 5632], P('sp', 'tp'), may hold values from -0.125 to 0.125
- mixer_down: bfloat16 [5632, 2048], P('tp', 'sp'), may hold values from -0.078125 to 0.078125
Outputs:
- layer_out: bfloat16 [20480, 2048], P(('grp', 'sp', 'tp')), parts along dimension 0
There are 2 independent parts, one for each index of `grp`. A program takes and returns all parts, laid end to end along the dimension named above; an argument that names none is the same for every part. Nothing has to cross between parts.
All inputs are finite; a program needn't handle non-finite values.
Results may differ from a plain program's by a relative error of at most 0.015.
The roundings to bfloat16 on the way count: a program that leaves them out, or rounds other values in their place, can miss the bound.
Values may be sent and summed in bfloat16 or wider, within the bound.
A program may use at most 128 MiB of HBM per device.

v0:
```python
import math

import jax
import jax.numpy as jnp
from jax import lax
from jax.sharding import PartitionSpec as P

GRID = 64


eps = 1e-06
theta = 10000.0


def gather_turned(arrays, axis, dims):
    turned = [jnp.moveaxis(a, dim, 0) for a, dim in zip(arrays, dims)]
    widths = [t[0].size for t in turned]
    both = jnp.concatenate([t.reshape(-1, w) for t, w in zip(turned, widths)], axis=1)
    whole = lax.all_gather(both, axis, axis=0, tiled=True)
    parts = jnp.split(whole, [sum(widths[:k]) for k in range(1, len(widths))], axis=1)
    return tuple(
        (
            jnp.moveaxis(b.reshape(-1, *t.shape[1:]), 0, dim)
            for b, t, dim in zip(parts, turned, dims)
        )
    )


def split_up(x, dim, count):
    before, after = (x.shape[:dim], x.shape[dim + 1 :])
    return jnp.moveaxis(x.reshape(*before, count, -1, *after), dim, 0)


def sum_at_owner(x, axis, dim):
    count = lax.axis_size(axis)
    parts = lax.all_to_all(split_up(x, dim, count), axis, 0, 0, tiled=True)
    return jnp.sum(parts.astype(jnp.float32), axis=0)


def sent_to_all(x, axis):
    count = lax.axis_size(axis)
    return lax.all_to_all(jnp.broadcast_to(x[None], (count, *x.shape)), axis, 0, 0, tiled=True)


def joined_along(parts, dim):
    dims = list(parts.shape[1:])
    dims[dim] *= parts.shape[0]
    return jnp.moveaxis(parts, 0, dim).reshape(dims)


def gathered_copies(x, axis, dim):
    parts = sent_to_all(x, axis)
    return joined_along(parts, dim)


def grid_angles(positions, width):
    quarter = width // 4
    freqs = theta ** (-jnp.arange(quarter, dtype=jnp.float32) * 4.0 / width)
    row = (positions // GRID).astype(jnp.float32)
    column = (positions % GRID).astype(jnp.float32)
    return jnp.concatenate(
        [row[:, None] * freqs[None, :], column[:, None] * freqs[None, :]], axis=-1
    )


def prepare(raw, gain, angles):
    field = raw.astype(jnp.float32)
    field = field * lax.rsqrt(jnp.mean(field * field, axis=-1, keepdims=True) + eps) * gain
    half = field.shape[-1] // 2
    cosine = jnp.cos(angles)[:, None, :]
    sine = jnp.sin(angles)[:, None, :]
    first = field[..., :half]
    second = field[..., half:]
    turned = jnp.concatenate(
        [first * cosine - second * sine, second * cosine + first * sine], axis=-1
    )
    return turned.astype(jnp.bfloat16)


def arrange(raw, gain, angles, key_heads, width):
    tokens = raw.shape[0]
    heads = raw.shape[1] // width
    queries = prepare(raw.reshape(tokens, heads, width), gain, angles)
    queries = queries.reshape(tokens, key_heads, heads // key_heads, width)
    return jnp.transpose(queries, (1, 2, 0, 3)).reshape(
        key_heads, heads // key_heads * tokens, width
    )


def own_keys(keyval, gain, angles, width):
    keys = prepare(keyval[:, :, :width], gain, angles)
    return jnp.concatenate([keys, keyval[:, :, width:]], axis=-1)


def block_extent(length):
    for extent in range(min(length, 2048), 0, -1):
        if length % extent == 0:
            return extent
    return 1


def absorb(state, keyval, queries, width):
    maxima, totals, summed = state
    keys = keyval[:, :, :width]
    values = keyval[:, :, width:]
    scores = jnp.einsum(
        "krd,skd->krs", queries, keys, preferred_element_type=jnp.float32
    ) / math.sqrt(width)
    peak = jnp.maximum(maxima, jnp.max(scores, axis=-1))
    rescale = jnp.exp(maxima - peak)
    weights = jnp.exp(scores - peak[..., None])
    totals = totals * rescale + jnp.sum(weights, axis=-1)
    summed = summed * rescale[..., None] + jnp.einsum(
        "krs,skd->krd", weights.astype(jnp.bfloat16), values, preferred_element_type=jnp.float32
    )
    return (peak, totals, summed)


def sweep(state, piece, queries, width):
    length = piece.shape[0]
    extent = block_extent(length)
    blocks = piece.reshape(length // extent, extent, piece.shape[1], piece.shape[2])

    def visit(carry, keyval):
        return (absorb(carry, keyval, queries, width), None)

    state, unused = lax.scan(visit, state, blocks)
    return state


def start_state(queries):
    rows_here = queries.shape[1]
    heads_here = queries.shape[0]
    return (
        jnp.full((heads_here, rows_here), -jnp.inf, jnp.float32),
        jnp.zeros((heads_here, rows_here), jnp.float32),
        jnp.zeros((heads_here, rows_here, queries.shape[2]), jnp.float32),
    )


def finish(state, groups, tokens):
    maxima, totals, summed = state
    attn = (summed / totals[..., None]).astype(jnp.bfloat16)
    return attn.reshape(attn.shape[0], groups, tokens, attn.shape[2])


def local(
    residual_in,
    narrow_query_rows,
    wide_query_rows,
    narrow_key_value,
    wide_key_value,
    narrow_norm_gains,
    wide_norm_gains,
    out_narrow,
    out_wide,
    mixer_gain,
    mixer_gate,
    mixer_up,
    mixer_down,
):
    gate_whole, up_whole, down_whole = gather_turned(
        (mixer_gate, mixer_up, mixer_down), "sp", (0, 0, 1)
    )
    tokens = narrow_query_rows.shape[0]
    narrow_width = narrow_key_value.shape[2] // 2
    wide_width = wide_key_value.shape[2] // 2
    narrow_heads = narrow_key_value.shape[1]
    wide_heads = wide_key_value.shape[1]
    positions = lax.axis_index("sp") * tokens + jnp.arange(tokens, dtype=jnp.int32)
    angles_narrow = grid_angles(positions, narrow_width)
    angles_wide = grid_angles(positions, wide_width)
    queries_narrow = arrange(
        narrow_query_rows, narrow_norm_gains[0], angles_narrow, narrow_heads, narrow_width
    )
    queries_wide = arrange(wide_query_rows, wide_norm_gains[0], angles_wide, wide_heads, wide_width)
    sent_narrow = own_keys(narrow_key_value, narrow_norm_gains[1], angles_narrow, narrow_width)
    sent_wide = own_keys(wide_key_value, wide_norm_gains[1], angles_wide, wide_width)
    state_narrow = sweep(
        start_state(queries_narrow),
        lax.all_gather(sent_narrow, "sp", axis=0, tiled=True),
        queries_narrow,
        narrow_width,
    )
    state_wide = sweep(
        start_state(queries_wide),
        lax.all_gather(sent_wide, "sp", axis=0, tiled=True),
        queries_wide,
        wide_width,
    )
    groups_narrow = queries_narrow.shape[1] // tokens
    groups_wide = queries_wide.shape[1] // tokens
    attention_narrow = finish(state_narrow, groups_narrow, tokens)
    attention_wide = finish(state_wide, groups_wide, tokens)
    weight_narrow = out_narrow.reshape(
        narrow_heads, groups_narrow, narrow_width, out_narrow.shape[1]
    )
    weight_wide = out_wide.reshape(wide_heads, groups_wide, wide_width, out_wide.shape[1])
    total = jnp.einsum(
        "kgtd,kgdn->tn", attention_narrow, weight_narrow, preferred_element_type=jnp.float32
    )
    attended = sum_at_owner(
        (
            total
            + jnp.einsum(
                "kgtd,kgdn->tn", attention_wide, weight_wide, preferred_element_type=jnp.float32
            )
        ).astype(jnp.bfloat16),
        "tp",
        0,
    ).astype(jnp.bfloat16)
    stream = residual_in.astype(jnp.float32) + attended.astype(jnp.float32)
    scale = lax.rsqrt(jnp.mean(stream * stream, axis=-1, keepdims=True) + eps)
    normed = (stream * scale * mixer_gain).astype(jnp.bfloat16)
    whole_rows = gathered_copies(normed, "tp", 0)
    gate = jnp.dot(whole_rows, gate_whole, preferred_element_type=jnp.float32)
    up = jnp.dot(whole_rows, up_whole, preferred_element_type=jnp.float32)
    hidden = (jax.nn.silu(gate) * up).astype(jnp.bfloat16)
    terms = jnp.dot(hidden, down_whole, preferred_element_type=jnp.float32)
    branch = sum_at_owner(terms.astype(jnp.bfloat16), "tp", 0).astype(jnp.bfloat16)
    return (stream + branch.astype(jnp.float32)).astype(jnp.bfloat16)


def solution(mesh):
    placed = (
        P(("grp", "sp", "tp"), None),
        P(("grp", "sp"), "tp"),
        P(("grp", "sp"), "tp"),
        P(("grp", "sp"), "tp", None),
        P(("grp", "sp"), "tp", None),
        P(),
        P(),
        P("tp", None),
        P("tp", None),
        P(),
        P("sp", "tp"),
        P("sp", "tp"),
        P("tp", "sp"),
    )
    return jax.shard_map(
        local, mesh=mesh, in_specs=placed, out_specs=P(("grp", "sp", "tp"), None), check_vma=False
    )
```

profile of v0, /device:TPU:33, one launch (start us, length us, event | category | flops | bytes accessed | tf_op | source)
XLA Modules:
  0.0 319.0 jit_solution(6801124048486298095)
XLA Ops:
  6.6 0.8 slice_bitcast_fusion.10
  7.4 1.0 fusion.86
  10.1 0.9 slice.72
  11.0 1.0 fusion.60
  12.1 0.8 slice_bitcast_fusion.8
  12.8 1.0 fusion.61
  14.7 0.8 pad_maximum_fusion.2
  15.6 2.0 pad_maximum_fusion
  21.4 73.9 %all-gather.4.cloned.1.call-done = bf16[10240,1,128]{2,0,1:T(8,128)(2,1)} async-done(((bf16[320,1,128]{2,0,1:T(8,128)(2,1)}), bf16[10240,1,128]{2,0,1:T(8,128)(2,1)}) %all-gather.4.cloned.1.call-update) | async-done | bytes 2621456 | tf_op jit(solution)/shard_map/all_gather | solution.py:181
  95.3 77.8 %while.30 = (s32[]{:T(128)}, f32[1,1280]{1,0:T(1,128)S(1)}, f32[1,1280]{1,0:T(1,128)S(1)}, f32[1,1280,64]{1,2,0:T(8,128)S(1)}, bf16[5,2048,1,128]{3,1,2,0:T(8,12...) while((s32[]{:T(128)}, f32[1,1280]{1,0:T(1,128)S(1)}, ...), condition=%wide.region_5.6_spmd.clone, body=%wide.region_2.5_spmd.clone.sunk | while | flops 692313600 | bytes 76403840 | solution.py:127
  95.3 1.1 dynamic-slice_bitcast_fusion.4
  96.4 5.5 %multiply_reduce_fusion.6 = (f32[1280]{0:T(1024)S(1)}, f32[2048,1280]{1,0:T(8,128)}) fusion(bf16[1,1280,64]{2,1,0:T(8,128)(2,1)S(1)} %get-tuple-element.370, bf16[2048,1,128]{2,0,1:T(8,128)(2,1)S(1)} %dynamic-slice_bitcast_fusion.4), kind=kOutput, calls=%fused_computation.1.clone.1 | convolution fusion | flops 340785920 | bytes 11179008 | tf_op jit(solution)/shard_map/while/body/eval_jaxpr/krd,skd->krs/dot_general | solution.py:106
  102.0 6.0 %fusion.106 = f32[1,1280,64]{1,2,0:T(8,128)S(1)} fusion(f32[2048,1280]{1,0:T(8,128)} %get-tuple-element.311, f32[1280]{0:T(1024)S(1)} %get-tuple-element.312, bf16[2048,1,128]{2,0,1:T(8,128)(2,1)S(1)} %dynamic-slice_bitcast_fusion.4, f32[1,1280,64]{1,2,0:T(8,128)S(1)} %get-tuple-element.360, f32[1280]{0:T(1024)S(1)} %get-tuple-element.313, ...), kind=kOutput, calls=%fused_computation.6.clone.1 | convolution fusion | flops 343654400 | bytes 11675649 | tf_op jit(solution)/shard_map/while/body/eval_jaxpr/krs,skd->krd/dot_general | solution.py:113
  108.0 1.0 copy-done.1
  108.9 1.8 fusion.104
  110.7 1.1 dynamic-slice_bitcast_fusion.4
  111.8 5.5 %multiply_reduce_fusion.6 = (f32[1280]{0:T(1024)S(1)}, f32[2048,1280]{1,0:T(8,128)}) fusion(bf16[1,1280,64]{2,1,0:T(8,128)(2,1)S(1)} %get-tuple-element.370, bf16[2048,1,128]{2,0,1:T(8,128)(2,1)S(1)} %dynamic-slice_bitcast_fusion.4), kind=kOutput, calls=%fused_computation.1.clone.1 | convolution fusion | flops 340785920 | bytes 11179008 | tf_op jit(solution)/shard_map/while/body/eval_jaxpr/krd,skd->krs/dot_general | solution.py:106
  117.4 6.1 %fusion.106 = f32[1,1280,64]{1,2,0:T(8,128)S(1)} fusion(f32[2048,1280]{1,0:T(8,128)} %get-tuple-element.311, f32[1280]{0:T(1024)S(1)} %get-tuple-element.312, bf16[2048,1,128]{2,0,1:T(8,128)(2,1)S(1)} %dynamic-slice_bitcast_fusion.4, f32[1,1280,64]{1,2,0:T(8,128)S(1)} %get-tuple-element.360, f32[1280]{0:T(1024)S(1)} %get-tuple-element.313, ...), kind=kOutput, calls=%fused_computation.6.clone.1 | convolution fusion | flops 343654400 | bytes 11675649 | tf_op jit(solution)/shard_map/while/body/eval_jaxpr/krs,skd->krd/dot_general | solution.py:113
  123.5 1.1 copy-done.1
  124.6 1.8 fusion.104
  126.4 1.1 dynamic-slice_bitcast_fusion.4
  127.5 5.5 %multiply_reduce_fusion.6 = (f32[1280]{0:T(1024)S(1)}, f32[2048,1280]{1,0:T(8,128)}) fusion(bf16[1,1280,64]{2,1,0:T(8,128)(2,1)S(1)} %get-tuple-element.370, bf16[2048,1,128]{2,0,1:T(8,128)(2,1)S(1)} %dynamic-slice_bitcast_fusion.4), kind=kOutput, calls=%fused_computation.1.clone.1 | convolution fusion | flops 340785920 | bytes 11179008 | tf_op jit(solution)/shard_map/while/body/eval_jaxpr/krd,skd->krs/dot_general | solution.py:106
  133.1 6.1 %fusion.106 = f32[1,1280,64]{1,2,0:T(8,128)S(1)} fusion(f32[2048,1280]{1,0:T(8,128)} %get-tuple-element.311, f32[1280]{0:T(1024)S(1)} %get-tuple-element.312, bf16[2048,1,128]{2,0,1:T(8,128)(2,1)S(1)} %dynamic-slice_bitcast_fusion.4, f32[1,1280,64]{1,2,0:T(8,128)S(1)} %get-tuple-element.360, f32[1280]{0:T(1024)S(1)} %get-tuple-element.313, ...), kind=kOutput, calls=%fused_computation.6.clone.1 | convolution fusion | flops 343654400 | bytes 11675649 | tf_op jit(solution)/shard_map/while/body/eval_jaxpr/krs,skd->krd/dot_general | solution.py:113
  139.2 1.1 copy-done.1
  140.3 1.8 fusion.104
  142.1 1.1 dynamic-slice_bitcast_fusion.4
  143.2 5.5 %multiply_reduce_fusion.6 = (f32[1280]{0:T(1024)S(1)}, f32[2048,1280]{1,0:T(8,128)}) fusion(bf16[1,1280,64]{2,1,0:T(8,128)(2,1)S(1)} %get-tuple-element.370, bf16[2048,1,128]{2,0,1:T(8,128)(2,1)S(1)} %dynamic-slice_bitcast_fusion.4), kind=kOutput, calls=%fused_computation.1.clone.1 | convolution fusion | flops 340785920 | bytes 11179008 | tf_op jit(solution)/shard_map/while/body/eval_jaxpr/krd,skd->krs/dot_general | solution.py:106
  148.8 6.1 %fusion.106 = f32[1,1280,64]{1,2,0:T(8,128)S(1)} fusion(f32[2048,1280]{1,0:T(8,128)} %get-tuple-element.311, f32[1280]{0:T(1024)S(1)} %get-tuple-element.312, bf16[2048,1,128]{2,0,1:T(8,128)(2,1)S(1)} %dynamic-slice_bitcast_fusion.4, f32[1,1280,64]{1,2,0:T(8,128)S(1)} %get-tuple-element.360, f32[1280]{0:T(1024)S(1)} %get-tuple-element.313, ...), kind=kOutput, calls=%fused_computation.6.clone.1 | convolution fusion | flops 343654400 | bytes 11675649 | tf_op jit(solution)/shard_map/while/body/eval_jaxpr/krs,skd->krd/dot_general | solution.py:113
  154.9 1.1 copy-done.1
  155.9 1.8 fusion.104
  157.7 1.1 dynamic-slice_bitcast_fusion.4
  158.8 5.5 %multiply_reduce_fusion.6 = (f32[1280]{0:T(1024)S(1)}, f32[2048,1280]{1,0:T(8,128)}) fusion(bf16[1,1280,64]{2,1,0:T(8,128)(2,1)S(1)} %get-tuple-element.370, bf16[2048,1,128]{2,0,1:T(8,128)(2,1)S(1)} %dynamic-slice_bitcast_fusion.4), kind=kOutput, calls=%fused_computation.1.clone.1 | convolution fusion | flops 340785920 | bytes 11179008 | tf_op jit(solution)/shard_map/while/body/eval_jaxpr/krd,skd->krs/dot_general | solution.py:106
  164.4 6.0 %fusion.106 = f32[1,1280,64]{1,2,0:T(8,128)S(1)} fusion(f32[2048,1280]{1,0:T(8,128)} %get-tuple-element.311, f32[1280]{0:T(1024)S(1)} %get-tuple-element.312, bf16[2048,1,128]{2,0,1:T(8,128)(2,1)S(1)} %dynamic-slice_bitcast_fusion.4, f32[1,1280,64]{1,2,0:T(8,128)S(1)} %get-tuple-element.360, f32[1280]{0:T(1024)S(1)} %get-tuple-element.313, ...), kind=kOutput, calls=%fused_computation.6.clone.1 | convolution fusion | flops 343654400 | bytes 11675649 | tf_op jit(solution)/shard_map/while/body/eval_jaxpr/krs,skd->krd/dot_general | solution.py:113
  170.4 1.0 copy-done.1
  171.4 1.8 fusion.104
  173.5 48.6 %while.31 = (s32[]{:T(128)}, f32[1,640]{1,0:T(1,128)S(1)}, f32[1,640]{1,0:T(1,128)S(1)}, f32[1,640,128]{2,1,0:T(8,128)S(1)}, bf16[5,2048,1,256]{3,1,2,0:T(8,128)...) while((s32[]{:T(128)}, f32[1,640]{1,0:T(1,128)S(1)}, ...), condition=%wide.region_11.12_spmd.clone, body=%wide.region_8.11_spmd.clone.sunk | while | flops 681824000 | bytes 40711808 | solution.py:127
  173.5 1.3 dynamic-slice_bitcast_fusion.5
  174.8 3.2 multiply_reduce_fusion.7
  178.0 3.7 %fusion.111 = f32[1,640,128]{2,1,0:T(8,128)S(1)} fusion(f32[2048,640]{1,0:T(8,128)} %get-tuple-element.322, f32[640]{0:T(1024)S(1)} %get-tuple-element.323, bf16[2048,1,256]{2,0,1:T(8,128)(2,1)S(1)} %dynamic-slice_bitcast_fusion.5, f32[1,640,128]{2,1,0:T(8,128)S(1)} %get-tuple-element.336, f32[640]{0:T(1024)S(1)} %get-tuple-element.324, ...), kind=kOutput, calls=%fused_computation.29.clone.1 | convolution fusion | flops 339722240 | bytes 6430721 | tf_op jit(solution)/shard_map/while/body/eval_jaxpr/krs,skd->krd/dot_general | solution.py:113
  182.4 0.9 fusion.109
  183.3 1.3 dynamic-slice_bitcast_fusion.5
  184.6 3.2 multiply_reduce_fusion.7
  187.8 3.8 %fusion.111 = f32[1,640,128]{2,1,0:T(8,128)S(1)} fusion(f32[2048,640]{1,0:T(8,128)} %get-tuple-element.322, f32[640]{0:T(1024)S(1)} %get-tuple-element.323, bf16[2048,1,256]{2,0,1:T(8,128)(2,1)S(1)} %dynamic-slice_bitcast_fusion.5, f32[1,640,128]{2,1,0:T(8,128)S(1)} %get-tuple-element.336, f32[640]{0:T(1024)S(1)} %get-tuple-element.324, ...), kind=kOutput, calls=%fused_computation.29.clone.1 | convolution fusion | flops 339722240 | bytes 6430721 | tf_op jit(solution)/shard_map/while/body/eval_jaxpr/krs,skd->krd/dot_general | solution.py:113
  192.1 0.9 fusion.109
  193.0 1.3 dynamic-slice_bitcast_fusion.5
  194.3 3.2 multiply_reduce_fusion.7
  197.5 3.8 %fusion.111 = f32[1,640,128]{2,1,0:T(8,128)S(1)} fusion(f32[2048,640]{1,0:T(8,128)} %get-tuple-element.322, f32[640]{0:T(1024)S(1)} %get-tuple-element.323, bf16[2048,1,256]{2,0,1:T(8,128)(2,1)S(1)} %dynamic-slice_bitcast_fusion.5, f32[1,640,128]{2,1,0:T(8,128)S(1)} %get-tuple-element.336, f32[640]{0:T(1024)S(1)} %get-tuple-element.324, ...), kind=kOutput, calls=%fused_computation.29.clone.1 | convolution fusion | flops 339722240 | bytes 6430721 | tf_op jit(solution)/shard_map/while/body/eval_jaxpr/krs,skd->krd/dot_general | solution.py:113
  201.8 0.9 fusion.109
  202.7 1.3 dynamic-slice_bitcast_fusion.5
  204.0 3.2 multiply_reduce_fusion.7
  207.2 3.8 %fusion.111 = f32[1,640,128]{2,1,0:T(8,128)S(1)} fusion(f32[2048,640]{1,0:T(8,128)} %get-tuple-element.322, f32[640]{0:T(1024)S(1)} %get-tuple-element.323, bf16[2048,1,256]{2,0,1:T(8,128)(2,1)S(1)} %dynamic-slice_bitcast_fusion.5, f32[1,640,128]{2,1,0:T(8,128)S(1)} %get-tuple-element.336, f32[640]{0:T(1024)S(1)} %get-tuple-element.324, ...), kind=kOutput, calls=%fused_computation.29.clone.1 | convolution fusion | flops 339722240 | bytes 6430721 | tf_op jit(solution)/shard_map/while/body/eval_jaxpr/krs,skd->krd/dot_general | solution.py:113
  211.4 0.9 fusion.109
  212.4 1.3 dynamic-slice_bitcast_fusion.5
  213.7 3.2 multiply_reduce_fusion.7
  217.0 3.8 %fusion.111 = f32[1,640,128]{2,1,0:T(8,128)S(1)} fusion(f32[2048,640]{1,0:T(8,128)} %get-tuple-element.322, f32[640]{0:T(1024)S(1)} %get-tuple-element.323, bf16[2048,1,256]{2,0,1:T(8,128)(2,1)S(1)} %dynamic-slice_bitcast_fusion.5, f32[1,640,128]{2,1,0:T(8,128)S(1)} %get-tuple-element.336, f32[640]{0:T(1024)S(1)} %get-tuple-element.324, ...), kind=kOutput, calls=%fused_computation.29.clone.1 | convolution fusion | flops 339722240 | bytes 6430721 | tf_op jit(solution)/shard_map/while/body/eval_jaxpr/krs,skd->krd/dot_general | solution.py:113
  221.2 0.9 fusion.109
  222.9 1.8 fusion.47
  224.7 21.2 %all_to_all.15 = bf16[4,80,2048]{2,1,0:T(8,128)(2,1)S(1)} all-to-all(bf16[4,80,2048]{2,1,0:T(8,128)(2,1)S(1)} %bitcast.124), channel_id=1, replica_groups=mesh['grp'=2,'sp'=32,'tp'=4] {'tp'}, dimensions={0} | all-to-all | bytes 2621440 | tf_op jit(solution)/shard_map/all_to_all | solution.py:36
  246.7 18.8 %all_to_all.16 = bf16[4,80,2048]{2,1,0:T(8,128)(2,1)S(1)} all-to-all(bf16[4,80,2048]{2,1,0:T(8,128)(2,1)S(1)} %broadcast_in_dim.20), channel_id=1, replica_groups=mesh['grp'=2,'sp'=32,'tp'=4] {'tp'}, dimensions={0} | all-to-all | bytes 2621440 | tf_op jit(solution)/shard_map/all_to_all | solution.py:42
  265.5 8.1 %all-gather.8.cloned.1.call-done = bf16[2048,4224]{1,0:T(8,128)(2,1)} async-done(((bf16[64,4224]{1,0:T(8,128)(2,1)}), bf16[2048,4224]{1,0:T(8,128)(2,1)}) %all-gather.8.cloned.1.call-update) | async-done | bytes 17301520 | tf_op jit(solution)/shard_map/all_gather | solution.py:19
  273.7 6.1 %fusion.38 = f32[320,1408]{1,0:T(8,128)} fusion(bf16[320,2048]{1,0:T(8,128)(2,1)S(1)} %bitcast.126, bf16[2048,4224]{1,0:T(8,128)(2,1)} %all-gather.8.cloned.1.call-done), kind=kOutput, calls=%fused_computation.48 | convolution fusion | flops 1845493760 | bytes 8880128 | tf_op jit(solution)/shard_map/dot_general | solution.py:216
  279.7 10.2 %fusion.44 = bf16[320,2048]{1,0:T(8,128)(2,1)} fusion(bf16[2048,4224]{1,0:T(8,128)(2,1)} %all-gather.8.cloned.1.call-done, bf16[320,2048]{1,0:T(8,128)(2,1)S(1)} %bitcast.127, f32[320,1408]{1,0:T(8,128)} %fusion.38), kind=kOutput, calls=%fused_computation.54 | convolution fusion | flops 3694346240 | bytes 15958016 | tf_op jit(solution)/shard_map/dot_general | solution.py:219
  289.9 21.4 %all_to_all.17 = bf16[4,80,2048]{2,1,0:T(8,128)(2,1)S(1)} all-to-all(bf16[4,80,2048]{2,1,0:T(8,128)(2,1)} %bitcast.128), channel_id=1, replica_groups=mesh['grp'=2,'sp'=32,'tp'=4] {'tp'}, dimensions={0} | all-to-all | bytes 2621440 | tf_op jit(solution)/shard_map/all_to_all | solution.py:36
  311.6 0.8 add_convert_fusion
  (111 shorter events, 11.0 us)
Async XLA Ops:
  6.5 215.8 %copy-start = (bf16[256,2048]{1,0:T(8,128)(2,1)S(1)}, bf16[256,2048]{1,0:T(8,128)(2,1)}, u32[]{:S(2)}) copy-start(bf16[256,2048]{1,0:T(8,128)(2,1)} %param.25) | copy-start | bytes 3145732
  6.6 11.2 %copy-start.4 = (bf16[320,256]{1,0:T(8,128)(2,1)S(1)}, bf16[320,256]{1,0:T(8,128)(2,1)}, u32[]{:S(2)}) copy-start(bf16[320,256]{1,0:T(8,128)(2,1)} %param.18) | copy-start | bytes 491524
  6.6 12.0 %copy-start.5 = (bf16[320,256]{1,0:T(8,128)(2,1)S(1)}, bf16[320,256]{1,0:T(8,128)(2,1)}, u32[]{:S(2)}) copy-start(bf16[320,256]{1,0:T(8,128)(2,1)} %param.19) | copy-start | bytes 491524
  6.6 88.8 %all-gather.4.cloned.1.call-start = ((), (), s32[]{:S(2)}) async-start(), calls=%async_computation.3 | async-start | bytes 2703360 | tf_op jit(solution)/shard_map/all_gather | solution.py:181
  10.0 163.4 %all-gather.6.cloned.1.call-start = ((), (), s32[]{:S(2)}) async-start(), calls=%async_computation.4 | async-start | bytes 5406720 | tf_op jit(solution)/shard_map/all_gather | solution.py:187
  15.6 258.1 %all-gather.8.cloned.1.call-start = ((), (), s32[]{:S(2)}) async-start(), calls=%async_computation.5 | async-start | bytes 17842176 | tf_op jit(solution)/shard_map/all_gather | solution.py:19
  102.0 7.0 %copy-start.1 = (f32[2048,1280]{1,0:T(8,128)S(1)}, f32[2048,1280]{1,0:T(8,128)}, u32[]{:S(2)}) copy-start(f32[2048,1280]{1,0:T(8,128)} %get-tuple-element.311) | copy-start | bytes 31457284 | tf_op jit(solution)/shard_map/while
  117.4 7.2 %copy-start.1 = (f32[2048,1280]{1,0:T(8,128)S(1)}, f32[2048,1280]{1,0:T(8,128)}, u32[]{:S(2)}) copy-start(f32[2048,1280]{1,0:T(8,128)} %get-tuple-element.311) | copy-start | bytes 31457284 | tf_op jit(solution)/shard_map/while
  133.1 7.2 %copy-start.1 = (f32[2048,1280]{1,0:T(8,128)S(1)}, f32[2048,1280]{1,0:T(8,128)}, u32[]{:S(2)}) copy-start(f32[2048,1280]{1,0:T(8,128)} %get-tuple-element.311) | copy-start | bytes 31457284 | tf_op jit(solution)/shard_map/while
  148.7 7.2 %copy-start.1 = (f32[2048,1280]{1,0:T(8,128)S(1)}, f32[2048,1280]{1,0:T(8,128)}, u32[]{:S(2)}) copy-start(f32[2048,1280]{1,0:T(8,128)} %get-tuple-element.311) | copy-start | bytes 31457284 | tf_op jit(solution)/shard_map/while
  164.4 7.0 %copy-start.1 = (f32[2048,1280]{1,0:T(8,128)S(1)}, f32[2048,1280]{1,0:T(8,128)}, u32[]{:S(2)}) copy-start(f32[2048,1280]{1,0:T(8,128)} %get-tuple-element.311) | copy-start | bytes 31457284 | tf_op jit(solution)/shard_map/while
  178.0 4.4 %copy-start.2 = (f32[2048,640]{1,0:T(8,128)S(1)}, f32[2048,640]{1,0:T(8,128)}, u32[]{:S(2)}) copy-start(f32[2048,640]{1,0:T(8,128)} %get-tuple-element.322) | copy-start | bytes 15728644 | tf_op jit(solution)/shard_map/while
  187.8 4.3 %copy-start.2 = (f32[2048,640]{1,0:T(8,128)S(1)}, f32[2048,640]{1,0:T(8,128)}, u32[]{:S(2)}) copy-start(f32[2048,640]{1,0:T(8,128)} %get-tuple-element.322) | copy-start | bytes 15728644 | tf_op jit(solution)/shard_map/while
  197.5 4.2 %copy-start.2 = (f32[2048,640]{1,0:T(8,128)S(1)}, f32[2048,640]{1,0:T(8,128)}, u32[]{:S(2)}) copy-start(f32[2048,640]{1,0:T(8,128)} %get-tuple-element.322) | copy-start | bytes 15728644 | tf_op jit(solution)/shard_map/while
  207.2 4.2 %copy-start.2 = (f32[2048,640]{1,0:T(8,128)S(1)}, f32[2048,640]{1,0:T(8,128)}, u32[]{:S(2)}) copy-start(f32[2048,640]{1,0:T(8,128)} %get-tuple-element.322) | copy-start | bytes 15728644 | tf_op jit(solution)/shard_map/while
  216.9 4.2 %copy-start.2 = (f32[2048,640]{1,0:T(8,128)S(1)}, f32[2048,640]{1,0:T(8,128)}, u32[]{:S(2)}) copy-start(f32[2048,640]{1,0:T(8,128)} %get-tuple-element.322) | copy-start | bytes 15728644 | tf_op jit(solution)/shard_map/while
  222.8 23.3 %copy-start.3 = (bf16[80,2048]{1,0:T(8,128)(2,1)S(1)}, bf16[80,2048]{1,0:T(8,128)(2,1)}, u32[]{:S(2)}) copy-start(bf16[80,2048]{1,0:T(8,128)(2,1)} %param.17) | copy-start | bytes 983044
  222.9 23.6 %copy-start.6 = (f32[2048]{0:T(1024)S(1)}, f32[2048]{0:T(1024)}, u32[]{:S(2)}) copy-start(f32[2048]{0:T(1024)} %param.26) | copy-start | bytes 24580
Sparse Core Ops, SparseCore 0:
  10.2 85.0 all-gather.3
  97.2 70.0 all-gather.5
  169.1 104.4 all-gather.7
where the time goes:
time: 320 us; the launch traced here: 319 us
  matrix products  111 us (35%)
  waiting for transfers between devices  82.2 us (26%)
  blocking collectives  61.5 us (19%)
  other arithmetic  25.6 us (8%)
  local copies, waits for them, and re-layouts  24.2 us (8%)
  between operations  13.5 us (4%)
    all_gather x1, waiting for transfers between devices, local(): lax.all_gather(sent_narrow, 'sp', axis=0, tiled=True)  73.9 us
    dot_general x10, matrix products, absorb(): jnp.einsum('krs,skd->krd', weights.astype(jnp.bfloat16), values, preferre...  49.2 us
    dot_general x10, matrix products, absorb(): jnp.einsum('krd,skd->krs', queries, keys, preferred_element_type=jnp.floa...  43.6 us
    all_to_all x2, blocking collectives, sum_at_owner(): parts = lax.all_to_all(split_up(x, dim, count), axis, 0, 0, tiled=True)  42.7 us
    all_to_all x1, blocking collectives, sent_to_all(): lax.all_to_all(jnp.broadcast_to(x[None], (count, *x.shape)), axis, 0, 0,...  18.8 us
    reduce_sum x10, other arithmetic, absorb(): totals = totals * rescale + jnp.sum(weights, axis=-1)  13.4 us
    squeeze x10, local copies, waits for them, and re-layouts, sweep(): state, unused = lax.scan(visit, state, blocks)  12 us
    dot_general x1, matrix products, local(): terms = jnp.dot(hidden, down_whole, preferred_element_type=jnp.float32)  10.2 us
  transfers between devices with their start and end apart: 3, of which 2 were waited for; matrix products, arithmetic and copies ran while one was open for 42% of the time, Pallas kernels for 0%

commit v1 on v0

v1 whole, which is shorter than its diff:
```python
import functools
import math

import jax
import jax.numpy as jnp
import numpy as np
from jax import lax
from jax.experimental import pallas as pl
from jax.experimental.pallas import tpu as pltpu
from jax.sharding import PartitionSpec as P

GRID = 64
EPS = 1e-06
THETA = 10000.0
MESH = pl.DeviceIdType.MESH
F32 = jnp.float32
BF16 = jnp.bfloat16
CHUNKS = 4
PAD = 16


def nt(a, b):
    return lax.dot_general(a, b, (((1,), (1,)), ((), ())), preferred_element_type=F32)


def nn(a, b):
    return jnp.dot(a, b, preferred_element_type=F32)


def turn_tables(start, tokens, width):
    quarter = width // 4
    freqs = THETA ** (-jnp.arange(quarter, dtype=F32) * 4.0 / width)
    positions = start + jnp.arange(tokens, dtype=jnp.int32)
    row = (positions // GRID).astype(F32)
    column = (positions % GRID).astype(F32)
    angles = jnp.concatenate([row[:, None] * freqs[None], column[:, None] * freqs[None]], axis=-1)
    cosine, sine = jnp.cos(angles), jnp.sin(angles)
    return jnp.concatenate([cosine, cosine, -sine, sine], axis=-1)


def prepared(raw, gain, table):
    width = raw.shape[1]
    field = raw.astype(F32)
    field = field * lax.rsqrt(jnp.mean(field * field, axis=-1, keepdims=True) + EPS) * gain
    swapped = jnp.concatenate([field[:, width // 2 :], field[:, : width // 2]], axis=1)
    return (field * table[:, :width] + swapped * table[:, width:]).astype(BF16)


class Group:
    def __init__(self, whole, queries, peak, summed, width, tile):
        self.whole, self.queries, self.peak, self.summed = whole, queries, peak, summed
        self.width, self.tile = width, tile

    def start(self):
        self.peak[...] = jnp.full(self.peak.shape, -1e30, F32)
        self.summed[...] = jnp.zeros(self.summed.shape, F32)

    def absorb(self, slot):
        width = self.width
        cores, tokens, columns = self.whole.shape[1:]
        block = self.whole[slot].reshape(cores * tokens, columns)
        if width % 128:
            keys, values = block, block.T[width:]
        else:
            keys, values = block[:, :width], block[:, width:].T
        ones = jnp.ones((PAD, cores * tokens), BF16)
        values = jnp.concatenate([ones, values], axis=0)
        factor = math.log2(math.e) / math.sqrt(width)
        total = self.queries.shape[0]
        for low in range(0, total, self.tile):
            span = slice(low, min(low + self.tile, total))
            scores = nt(keys, self.queries[span, :])
            old = self.peak[:, span]
            new = jnp.maximum(old, jnp.max(scores, axis=0, keepdims=True))
            self.peak[:, span] = new
            weights = jnp.exp2((scores - new) * factor).astype(BF16)
            rescale = jnp.exp2((old - new) * factor)
            self.summed[:, span] = self.summed[:, span] * rescale + nn(values, weights)

    def finished(self):
        result = self.summed[PAD:, :] / self.summed[0:1, :]
        return result.T.astype(BF16)


def reduce_scatter(dest, part, relay, pair, direct, sems, axis, emit):
    send_a, send_b, send_c, recv_a, recv_b, recv_c = sems
    me = lax.axis_index(axis)
    right, left = lax.rem(me + 1, 4), lax.rem(me + 3, 4)
    far = lax.rem(me + 2, 4)

    def ways(c):
        return (right, left) if c % 2 == 0 else (left, right)

    def first(c):
        ahead, behind = ways(c)
        return (
            pltpu.make_async_remote_copy(
                part.at[c, far], relay.at[c], send_a.at[c], recv_a.at[c], dest(ahead), MESH
            ),
            pltpu.make_async_remote_copy(
                part.at[c, behind], direct.at[c], send_b.at[c], recv_b.at[c], dest(behind), MESH
            ),
        )

    def second(c):
        ahead, _ = ways(c)
        return pltpu.make_async_remote_copy(
            pair.at[c, 0], pair.at[c, 1], send_c.at[c], recv_c.at[c], dest(ahead), MESH
        )

    def forward(c):
        first(c)[0].wait_recv()
        ahead, _ = ways(c)
        pair[c, 0] = (part[c, ahead].astype(F32) + relay[c].astype(F32)).astype(BF16)
        second(c).start()

    for c in range(CHUNKS):
        emit(c)
        for copy in first(c):
            copy.start()
        if c:
            forward(c - 1)
    forward(CHUNKS - 1)
    sums = []
    for c in range(CHUNKS):
        first(c)[1].wait_recv()
        second(c).wait_recv()
        total = part[c, me].astype(F32) + direct[c].astype(F32) + pair[c, 1].astype(F32)
        sums.append(total.astype(BF16))
    for c in range(CHUNKS):
        for copy in (*first(c), second(c)):
            copy.wait_send()
    return sums


def attention_kernel(
    chips,
    nq, wq, nkv, wkv, ngain, wgain, ntable, wtable, outw, residual, mgain,
    stream_out, rows_out,
    gn, gw, qn, qw, npeak, wpeak, nsum, wsum, attn, part, relay, pair, direct, rows,
    ring_send, ring_recv, mate_send, mate_recv,
    rs_sems, ag_send, ag_recv,
):
    sp, tp = lax.axis_index("sp"), lax.axis_index("tp")
    count = 2 * chips
    core = lax.rem(sp, 2)
    mate = sp + 1 - 2 * core
    up, down = lax.rem(sp + 2, count), lax.rem(sp + count - 2, count)
    right, left, across = lax.rem(tp + 1, 4), lax.rem(tp + 3, 4), lax.rem(tp + 2, 4)
    half = chips // 2
    tokens = nq.shape[0]
    nwidth, wwidth = ngain.shape[1], wgain.shape[1]

    barrier = pltpu.get_barrier_semaphore()
    for where in ({"sp": up}, {"sp": down}, {"sp": mate}, {"tp": right}, {"tp": left}):
        pl.semaphore_signal(barrier, inc=1, device_id=where, device_id_type=MESH)

    wholes = (gn, gw)

    def ring(piece, way, slot, target, here=None):
        whole = wholes[piece]
        return pltpu.make_async_remote_copy(
            whole.at[slot, core],
            whole.at[target, core],
            ring_send.at[piece, way, slot],
            ring_recv.at[piece, target],
            {"sp": up if way == 0 else down},
            MESH,
        )

    def to_mate(piece, slot):
        whole = wholes[piece]
        return pltpu.make_async_remote_copy(
            whole.at[slot, core],
            whole.at[slot, core],
            mate_send.at[piece, slot],
            mate_recv.at[piece, slot],
            {"sp": mate},
            MESH,
        )

    def arrive(piece, slot):
        ring(piece, 0, slot, slot).wait_recv()

    gn[0, core] = jnp.concatenate(
        [prepared(nkv[:, :nwidth], ngain[1:2, :], ntable[...]), nkv[:, nwidth:]], axis=1
    )
    gw[0, core, :, :wwidth] = prepared(wkv[:, :wwidth], wgain[1:2, :], wtable[...])
    gw[0, core, :, wwidth:] = wkv[:, wwidth:]
    pl.semaphore_wait(barrier, 5)
    for piece in (0, 1):
        ring(piece, 0, 0, 1).start()
        ring(piece, 1, 0, half + 1).start()
        to_mate(piece, 0).start()

    zeros = jnp.zeros((tokens, qn.shape[1] - nwidth), BF16)
    for head in range(qn.shape[0] // tokens):
        raw = nq[:, head * nwidth : (head + 1) * nwidth]
        turned = prepared(raw, ngain[0:1, :], ntable[...])
        qn[head * tokens : (head + 1) * tokens, :] = jnp.concatenate([turned, zeros], axis=1)
    for head in range(qw.shape[0] // tokens):
        raw = wq[:, head * wwidth : (head + 1) * wwidth]
        qw[head * tokens : (head + 1) * tokens, :] = prepared(raw, wgain[0:1, :], wtable[...])
    narrow = Group(gn, qn, npeak, nsum, nwidth, 256)
    wide = Group(gw, qw, wpeak, wsum, wwidth, 256)
    narrow.start()
    wide.start()
    groups = (narrow, wide)

    def absorb(piece, step):
        def one(i, carry):
            slot = jnp.where(i == 0, step, half + step)
            to_mate(piece, slot).wait_recv()
            groups[piece].absorb(slot)
            return carry

        lax.fori_loop(0, jnp.where((step == 0) | (step == half), 1, 2), one, 0)

    def pass_on(piece, step):
        @pl.when(step < half)
        def _():
            arrive(piece, step)
            if piece == 1:
                ring(piece, 0, step, step + 1).start()
            else:

                @pl.when(step + 1 < half)
                def _():
                    ring(piece, 0, step, step + 1).start()

            to_mate(piece, step).start()
            arrive(piece, half + step)
            if piece == 0:
                ring(piece, 1, half + step, jnp.where(step + 1 < half, half + step + 1, half)).start()
            else:

                @pl.when(step + 1 < half)
                def _():
                    ring(piece, 1, half + step, half + step + 1).start()

            to_mate(piece, half + step).start()

        @pl.when(step == half)
        def _():
            arrive(piece, half)
            to_mate(piece, half).start()

    absorb(0, jnp.int32(0))

    def turn(step, carry):
        pass_on(0, step)
        absorb(1, step - 1)
        pass_on(1, step)
        absorb(0, step)
        return carry

    lax.fori_loop(1, half + 1, turn, 0)
    absorb(1, jnp.int32(half))

    narrow_rows, wide_rows = narrow.finished(), wide.finished()
    low = 0
    for result, width in ((narrow_rows, nwidth), (wide_rows, wwidth)):
        for head in range(result.shape[0] // tokens):
            attn[:, low : low + width] = result[head * tokens : (head + 1) * tokens]
            low += width

    chunk = part.shape[3]

    def emit(c):
        terms = nn(attn[...], outw[:, c * chunk : (c + 1) * chunk]).astype(BF16)
        part[c] = terms.reshape(part.shape[1:])

    def dest(j):
        return {"tp": j}

    sums = reduce_scatter(dest, part, relay, pair, direct, rs_sems, "tp", emit)
    stream = residual[...].astype(F32) + jnp.concatenate(sums, axis=1).astype(F32)
    stream_out[...] = stream
    scale = lax.rsqrt(jnp.mean(stream * stream, axis=-1, keepdims=True) + EPS)
    normed = (stream * scale * mgain[...]).astype(BF16)
    split = rows.shape[3]
    rows[0, tp] = normed[:, :split]
    rows[1, tp] = normed[:, split:]

    def gather(h, way, owner):
        return pltpu.make_async_remote_copy(
            rows.at[h, owner],
            rows.at[h, owner],
            ag_send.at[h, way, owner],
            ag_recv.at[h, owner],
            {"tp": right if way == 0 else left},
            MESH,
        )

    gather(0, 0, tp).start()
    gather(1, 1, tp).start()
    gather(1, 0, tp).start()
    gather(0, 1, tp).start()
    gather(0, 0, left).wait_recv()
    gather(0, 0, left).start()
    gather(1, 0, right).wait_recv()
    gather(1, 1, right).start()
    for h, owner in ((1, left), (0, right), (0, across), (1, across)):
        gather(h, 0, owner).wait_recv()
    for h in (0, 1):
        rows_out[h] = rows[h].reshape(rows_out.shape[1:])
    for h, way, owner in ((0, 0, tp), (1, 1, tp), (1, 0, tp), (0, 1, tp), (0, 0, left), (1, 1, right)):
        gather(h, way, owner).wait_send()

    def drain(step, carry):
        for piece in (0, 1):

            @pl.when((step < half) if piece == 1 else (step + 1 < half))
            def _():
                ring(piece, 0, step, step + 1).wait_send()

            back = jnp.where(step == 0, 0, half + step)

            @pl.when((step < half) if piece == 0 else (step + 1 < half))
            def _():
                ring(piece, 1, back, half).wait_send()

            to_mate(piece, step).wait_send()

            @pl.when((step > 0) & (step < half))
            def _():
                to_mate(piece, half + step).wait_send()

        return carry

    lax.fori_loop(0, half + 1, drain, 0)


def mixer_kernel(
    rows, stream, weights,
    out,
    held, hidden, part, relay, pair, direct, fetch, rs_sems,
):
    tp = lax.axis_index("tp")
    right, left = lax.rem(tp + 1, 4), lax.rem(tp + 3, 4)
    barrier = pltpu.get_barrier_semaphore()
    for j in (right, left):
        pl.semaphore_signal(barrier, inc=1, device_id={"tp": j}, device_id_type=MESH)
    units = hidden.shape[1]
    split = rows.shape[2]

    def load(i):
        span = pl.ds(pl.multiple_of(i * 128, 128), 128)
        return pltpu.make_async_copy(weights.at[:, span], held.at[:, span], fetch.at[i])

    blocks = units // 128

    def begin(i, carry):
        load(i).start()
        load(blocks + i).start()
        return carry

    def begin_down(i, carry):
        load(2 * blocks + i).start()
        return carry

    lax.fori_loop(0, blocks, begin, 0)
    lax.fori_loop(0, blocks, begin_down, 0)

    def visit(i, carry):
        load(i).wait()
        load(blocks + i).wait()
        gates = pl.ds(pl.multiple_of(i * 128, 128), 128)
        ups = pl.ds(pl.multiple_of(units + i * 128, 128), 128)
        both = jnp.concatenate([held[:, gates], held[:, ups]], axis=1)
        product = nn(rows[0], both[:split]) + nn(rows[1], both[split:])
        gate, up = product[:, :128], product[:, 128:]
        hidden[:, gates] = (gate / (1.0 + jnp.exp(-gate)) * up).astype(BF16)
        return carry

    lax.fori_loop(0, blocks, visit, 0)

    def arrive(i, carry):
        load(2 * blocks + i).wait()
        return carry

    lax.fori_loop(0, blocks, arrive, 0)
    pl.semaphore_wait(barrier, 2)
    chunk = part.shape[3]

    def emit(c):
        terms = nt(hidden[...], held[c * chunk : (c + 1) * chunk, 2 * units :]).astype(BF16)
        part[c] = terms.reshape(part.shape[1:])

    def dest(j):
        return {"tp": j}

    sums = reduce_scatter(dest, part, relay, pair, direct, rs_sems, "tp", emit)
    out[...] = (stream[...] + jnp.concatenate(sums, axis=1).astype(F32)).astype(BF16)


def scatter_scratch(tokens, owned, chunk):
    return [
        pltpu.VMEM((CHUNKS, tokens // owned, owned, chunk), BF16),
        pltpu.VMEM((CHUNKS, owned, chunk), BF16),
        pltpu.VMEM((CHUNKS, 2, owned, chunk), BF16),
        pltpu.VMEM((CHUNKS, owned, chunk), BF16),
    ]


def scatter_sems():
    return [pltpu.SemaphoreType.DMA((CHUNKS,))] * 6


def local(
    chips,
    residual_in,
    narrow_query_rows,
    wide_query_rows,
    narrow_key_value,
    wide_key_value,
    narrow_norm_gains,
    wide_norm_gains,
    out_narrow,
    out_wide,
    mixer_gain,
    mixer_gate,
    mixer_up,
    mixer_down,
):
    shard = jnp.concatenate([mixer_gate, mixer_up, mixer_down.T], axis=1)
    weights = lax.all_gather(shard, "sp", axis=0, tiled=True)

    tokens = narrow_query_rows.shape[0]
    owned, model = residual_in.shape
    nkv = narrow_key_value.reshape(tokens, -1)
    wkv = wide_key_value.reshape(tokens, -1)
    nwidth, wwidth = nkv.shape[1] // 2, wkv.shape[1] // 2
    nrows = narrow_query_rows.shape[1] // nwidth * tokens
    wrows = wide_query_rows.shape[1] // wwidth * tokens
    start = lax.axis_index("sp") * tokens
    ntable = turn_tables(start, tokens, nwidth)
    wtable = turn_tables(start, tokens, wwidth)
    outw = jnp.concatenate([out_narrow, out_wide], axis=0)
    chunk = model // CHUNKS
    vmem = pl.BlockSpec(memory_space=pltpu.VMEM)
    DMA = pltpu.SemaphoreType.DMA

    stream, rows = pl.pallas_call(
        functools.partial(unpacked_attention, chips),
        out_shape=(
            jax.ShapeDtypeStruct((owned, model), F32),
            jax.ShapeDtypeStruct((2, tokens, model // 2), BF16),
        ),
        in_specs=[vmem] * 11,
        out_specs=(vmem, vmem),
        scratch_shapes=[
            pltpu.VMEM((chips, 2, tokens, nkv.shape[1]), BF16),
            pltpu.VMEM((chips, 2, tokens, wkv.shape[1]), BF16),
            pltpu.VMEM((nrows, nkv.shape[1]), BF16),
            pltpu.VMEM((wrows, wwidth), BF16),
            pltpu.VMEM((1, nrows), F32),
            pltpu.VMEM((1, wrows), F32),
            pltpu.VMEM((PAD + nwidth, nrows), F32),
            pltpu.VMEM((PAD + wwidth, wrows), F32),
            pltpu.VMEM((tokens, outw.shape[0]), BF16),
            *scatter_scratch(tokens, owned, chunk),
            pltpu.VMEM((2, tokens // owned, owned, model // 2), BF16),
            DMA((2, 2, chips)),
            DMA((2, chips)),
            DMA((2, chips)),
            DMA((2, chips)),
            *scatter_sems(),
            DMA((2, 2, tokens // owned)),
            DMA((2, tokens // owned)),
        ],
        compiler_params=pltpu.CompilerParams(
            collective_id=0, has_side_effects=True, vmem_limit_bytes=48 * 2**20
        ),
        cost_estimate=pl.CostEstimate(
            flops=60_000_000_000, bytes_accessed=10_000_000, transcendentals=20_000_000
        ),
        name="attend",
    )(
        narrow_query_rows,
        wide_query_rows,
        nkv,
        wkv,
        narrow_norm_gains,
        wide_norm_gains,
        ntable,
        wtable,
        outw,
        residual_in,
        mixer_gain.reshape(1, -1),
    )

    units = mixer_gate.shape[1]
    return pl.pallas_call(
        unpacked_mixer,
        out_shape=jax.ShapeDtypeStruct((owned, model), BF16),
        in_specs=[vmem, vmem, pl.BlockSpec(memory_space=pl.ANY)],
        out_specs=vmem,
        scratch_shapes=[
            pltpu.VMEM((model, 3 * units), BF16),
            pltpu.VMEM((tokens, units), BF16),
            *scatter_scratch(tokens, owned, chunk),
            DMA((3 * units // 128,)),
            *scatter_sems(),
        ],
        compiler_params=pltpu.CompilerParams(
            collective_id=1, has_side_effects=True, vmem_limit_bytes=48 * 2**20
        ),
        cost_estimate=pl.CostEstimate(
            flops=6_000_000_000, bytes_accessed=20_000_000, transcendentals=500_000
        ),
        name="mix",
    )(rows, stream, weights)


def unpacked_attention(chips, *refs):
    head, sems = refs[:31], refs[31:]
    attention_kernel(chips, *head, sems[0:6], sems[6], sems[7])


def unpacked_mixer(*refs):
    mixer_kernel(*refs[:11], refs[11:])


def solution(mesh):
    placed = (
        P(("grp", "sp", "tp"), None),
        P(("grp", "sp"), "tp"),
        P(("grp", "sp"), "tp"),
        P(("grp", "sp"), "tp", None),
        P(("grp", "sp"), "tp", None),
        P(),
        P(),
        P("tp", None),
        P("tp", None),
        P(),
        P("sp", "tp"),
        P("sp", "tp"),
        P("tp", "sp"),
    )
    return jax.shard_map(
        functools.partial(local, mesh.shape["sp"] // 2),
        mesh=mesh,
        in_specs=placed,
        out_specs=P(("grp", "sp", "tp"), None),
        check_vma=False,
    )
```

time: 320 us -> 198 us (0.62)
  Pallas kernels: 0 us -> 155 us
  matrix products: 111 us -> 0 us
  blocking collectives: 61.5 us -> 0 us
  waiting for transfers between devices: 82.2 us -> 22.1 us
  local copies, waits for them, and re-layouts: 24.2 us -> 1.94 us
  other arithmetic: 25.6 us -> 3.58 us
    pallas_call x0 -> x2, Pallas kernels: none -> 155 us  [the longest x1 134 us: local(): pl.pallas_call(functools.partial(unpacked_attention, chips), out_shape=(j...]
    dot_general x24 -> x0, matrix products: 111 us -> none  [the longest x10 49.2 us: absorb(): jnp.einsum('krs,skd->krd', weights.astype(jnp.bfloat16), values, preferre...]
    all_to_all x3 -> x0, blocking collectives: 61.5 us -> none  [the longest x2 42.7 us: sum_at_owner(): parts = lax.all_to_all(split_up(x, dim, count), axis, 0, 0, tiled=True)]
    all_gather x3 -> x1, waiting for transfers between devices: 82.1 us -> 22 us  [local(): weights = lax.all_gather(shard, 'sp', axis=0, tiled=True)]
    reduce_sum x17 -> x0, other arithmetic: 15.6 us -> none  [the longest x10 13.4 us: absorb(): totals = totals * rescale + jnp.sum(weights, axis=-1)]
    squeeze x10 -> x0, local copies, waits for them, and re-layouts: 12 us -> none  [sweep(): state, unused = lax.scan(visit, state, blocks)]
    while x30 -> x0, local copies, waits for them, and re-layouts: 7.44 us -> none
  transfers between devices with their start and end apart: 3 -> 1, of which waited for: 2 -> 1; matrix products, arithmetic and copies ran while one was open for 42% -> 1% of each run, Pallas kernels for 0% -> 68%
where the time goes in v1:
time: 198 us; the launch traced here: 196 us
  Pallas kernels  155 us (78%)
  waiting for transfers between devices  22.1 us (11%)
  between operations  13.6 us (7%)
  other arithmetic  3.58 us (2%)
    pallas_call x1, Pallas kernels, local(): pl.pallas_call(functools.partial(unpacked_attention, chips), out_shape=(j...  134 us
    all_gather x1, waiting for transfers between devices, local(): weights = lax.all_gather(shard, 'sp', axis=0, tiled=True)  22 us
    pallas_call x1, Pallas kernels, local(): pl.pallas_call(unpacked_mixer, out_shape=jax.ShapeDtypeStruct((owned, mod...  20.8 us
  transfers between devices with their start and end apart: 1, of which 1 were waited for; matrix products, arithmetic and copies ran while one was open for 1% of the time, Pallas kernels for 68%

profile of v1, /device:TPU:33, one launch (start us, length us, event | category | flops | bytes accessed | tf_op | source)
XLA Modules:
  0.0 196.4 jit_solution(11300484396346236393)
XLA Ops:
  6.5 0.0 all-gather.2.cloned.1.call-start
  6.6 1.9 pad_maximum_fusion.1
  8.5 0.0 copy-start.8
  8.5 0.0 copy-start.9
  8.5 0.1 all-gather.2.cloned.1.call-update
  8.6 0.1 broadcast_multiply_fusion.3
  8.7 0.2 fusion.3
  8.9 0.1 copy.16
  9.0 0.1 copy.17
  9.1 0.2 pad_maximum_fusion.3.refs_6_
  9.3 0.1 broadcast_multiply_fusion.1
  9.5 0.7 fusion.9
  10.1 0.2 pad_maximum_fusion.2.refs_7_
  10.3 0.0 copy-done.8
  10.4 0.0 copy-done.9
  10.4 0.0 copy-start
  10.4 0.0 copy-start.1
  10.4 0.0 copy-start.2
  10.4 0.0 copy-start.3
  10.4 0.0 copy-start.4
  10.4 0.0 copy-start.5
  10.4 0.0 copy-start.6
  10.4 0.0 copy-start.7
  10.5 0.1 pad_maximum_fusion.refs_8_
  10.6 0.7 copy-done
  11.3 0.0 copy-done.1
  11.4 0.1 copy-done.2
  11.5 0.1 copy-done.3
  11.5 0.0 copy-done.4
  11.6 0.0 copy-done.5
  11.6 0.0 copy-done.6
  11.6 0.0 copy-done.7
  11.6 134.4 %attend.1 = (f32[80,2048]{1,0:T(8,128)S(1)}, bf16[2,320,1024]{2,1,0:T(8,128)(2,1)S(1)}) custom-call(bf16[320,256]{1,0:T(8,128)(2,1)S(1)} %copy-done.1, bf16[320,256]{1,0:T(8,128)(2,1)S(1)} %copy-done.2, bf16[320,128]{1,0:T(8,128)(2,1)S(1)} %bitcast.5, bf16[320,256]{1,0:T(8,128)(2,1)S(1)} %bitcast.4, f32[2,64]{1,0:T(2,128)S(1)} %copy-done.6, ...), custom_call_target="tpu_custom_call" | custom-call | flops 60000002048 | bytes 10000000 | tf_op jit(solution)/shard_map/attend/pallas_call | solution.py:444
  146.0 22.0 %all-gather.2.cloned.1.call-done.refs_2_ = bf16[2048,4224]{1,0:T(8,128)(2,1)} async-done(((bf16[64,4224]{1,0:T(8,128)(2,1)}), bf16[2048,4224]{1,0:T(8,128)(2,1)}) %all-gather.2.cloned.1.call-update) | async-done | bytes 17301520 | tf_op jit(solution)/shard_map/all_gather | solution.py:427
  168.0 20.8 %mix.1 = bf16[80,2048]{1,0:T(8,128)(2,1)S(1)} custom-call(bf16[2,320,1024]{2,1,0:T(8,128)(2,1)S(1)} %get-tuple-element.7.refs_0_, f32[80,2048]{1,0:T(8,128)S(1)} %get-tuple-element.8.refs_1_, bf16[2048,4224]{1,0:T(8,128)(2,1)} %all-gather.2.cloned.1.call-done.refs_2_), custom_call_target="tpu_custom_call" | custom-call | flops 6000000000 | bytes 20000000 | tf_op jit(solution)/shard_map/mix/pallas_call | solution.py:494
  188.9 0.7 copy.21
  (4 shorter events, 0.0 us)
Async XLA Ops:
  6.5 161.5 %all-gather.2.cloned.1.call-start = ((), (), s32[]{:S(2)}) async-start(), calls=%async_computation | async-start | bytes 17842176 | tf_op jit(solution)/shard_map/all_gather | solution.py:427
  8.5 1.9 copy-start.8
  8.5 1.9 copy-start.9
  10.4 1.0 copy-start
  10.4 1.0 copy-start.1
  10.4 1.1 copy-start.2
  10.4 1.1 copy-start.3
  10.4 1.2 copy-start.4
  10.4 1.1 copy-start.5
  10.4 1.1 copy-start.6
  10.4 1.1 copy-start.7
Sparse Core Ops, SparseCore 0:
  9.2 158.7 all-gather.1

commit v2 on v1

v2 whole, which is shorter than its diff:
```python
import functools
import math

import jax
import jax.numpy as jnp
import numpy as np
from jax import lax
from jax.experimental import pallas as pl
from jax.experimental.pallas import tpu as pltpu
from jax.sharding import PartitionSpec as P

GRID = 64
EPS = 1e-06
THETA = 10000.0
MESH = pl.DeviceIdType.MESH
F32 = jnp.float32
BF16 = jnp.bfloat16
CHUNKS = 4
PAD = 16


def nt(a, b):
    return lax.dot_general(a, b, (((1,), (1,)), ((), ())), preferred_element_type=F32)


def nn(a, b):
    return jnp.dot(a, b, preferred_element_type=F32)


def frequencies(*widths):
    lanes, rows = [], []
    for width in widths:
        quarter = width // 4
        freqs = np.float32(THETA) ** (-np.arange(quarter, dtype=np.float32) * np.float32(4.0 / width))
        lanes += [freqs, freqs]
        rows += [np.ones(quarter), np.zeros(quarter)]
    lanes, rows = np.concatenate(lanes), np.concatenate(rows)
    spare = -len(lanes) % 128
    return np.pad(np.stack([lanes, rows]), ((0, 6), (0, spare))).astype(np.float32)


def prepared(raw, gain, table):
    width = raw.shape[1]
    field = raw.astype(F32)
    field = field * lax.rsqrt(jnp.mean(field * field, axis=-1, keepdims=True) + EPS) * gain
    swapped = jnp.concatenate([field[:, width // 2 :], field[:, : width // 2]], axis=1)
    return (field * table[:, :width] + swapped * table[:, width:]).astype(BF16)


class Group:
    def __init__(self, whole, queries, peak, summed, width, tile):
        self.whole, self.queries, self.peak, self.summed = whole, queries, peak, summed
        self.width, self.tile = width, tile

    def start(self):
        self.peak[...] = jnp.full(self.peak.shape, -1e30, F32)
        self.summed[...] = jnp.zeros(self.summed.shape, F32)

    def split(self, slot):
        width = self.width
        cores, tokens, columns = self.whole.shape[1:]
        block = self.whole[slot].reshape(cores * tokens, columns)
        if width % 128:
            keys, values = block, block.T[width:]
        else:
            keys, values = block[:, :width], block[:, width:].T
        ones = jnp.ones((PAD, cores * tokens), BF16)
        return keys, jnp.concatenate([ones, values], axis=0)

    def absorb(self, slots):
        factor = math.log2(math.e) / math.sqrt(self.width)
        total = self.queries.shape[0]
        spans = [slice(low, min(low + self.tile, total)) for low in range(0, total, self.tile)]
        items = [(block, span) for block in map(self.split, slots) for span in spans]

        def score(item):
            (keys, _), span = item
            return nt(keys, self.queries[span, :])

        def add(values, weights, rescale, span):
            self.summed[:, span] = self.summed[:, span] * rescale + nn(values, weights)

        behind = None
        ahead = score(items[0])
        for i, ((_, values), span) in enumerate(items):
            scores = ahead
            if i + 1 < len(items):
                ahead = score(items[i + 1])
            if behind is not None:
                add(*behind)
            old = self.peak[:, span]
            new = jnp.maximum(old, jnp.max(scores, axis=0, keepdims=True))
            self.peak[:, span] = new
            weights = jnp.exp2((scores - new) * factor).astype(BF16)
            behind = (values, weights, jnp.exp2((old - new) * factor), span)
        add(*behind)

    def finished(self):
        result = self.summed[PAD:, :] / self.summed[0:1, :]
        return result.T.astype(BF16)


def reduce_scatter(dest, part, relay, pair, direct, sems, axis, emit, serve):
    send_a, send_b, send_c, recv_a, recv_b, recv_c = sems
    me = lax.axis_index(axis)
    right, left = lax.rem(me + 1, 4), lax.rem(me + 3, 4)
    far = lax.rem(me + 2, 4)

    def ways(c):
        return (right, left) if c % 2 == 0 else (left, right)

    def relayed(c):
        return pltpu.make_async_remote_copy(
            part.at[c, far], relay.at[c], send_a.at[c], recv_a.at[c], dest(ways(c)[0]), MESH
        )

    def straight(c):
        ahead, behind = ways(c)
        return pltpu.make_async_remote_copy(
            part.at[c, behind], direct.at[c], send_b.at[c], recv_b.at[c], dest(behind), MESH
        )

    def paired(c):
        return pltpu.make_async_remote_copy(
            pair.at[c, 0], pair.at[c, 1], send_c.at[c], recv_c.at[c], dest(ways(c)[0]), MESH
        )

    for c in range(CHUNKS):
        emit(c)
        relayed(c).start()
        straight(c).start()
        serve()
    for c in range(CHUNKS):
        relayed(c).wait_recv()
        ahead, _ = ways(c)
        pair[c, 0] = (part[c, ahead].astype(F32) + relay[c].astype(F32)).astype(BF16)
        paired(c).start()
        serve()
    sums = []
    for c in range(CHUNKS):
        straight(c).wait_recv()
        paired(c).wait_recv()
        total = part[c, me].astype(F32) + direct[c].astype(F32) + pair[c, 1].astype(F32)
        sums.append(total.astype(BF16))
    for c in range(CHUNKS):
        relayed(c).wait_send()
        straight(c).wait_send()
        paired(c).wait_send()
    return sums


def layer_kernel(
    chips,
    nq, wq, nkv, wkv, ngain, wgain, freqs, residual, mgain, down_shard,
    outn, outw, gate_shard, up_shard,
    out,
    ntable, wtable, weights, gn, gw, qn, qw, npeak, wpeak, nsum, wsum, attn, projection,
    part, relay, pair, direct, rows, hidden,
    ring_send, ring_recv, mate_send, mate_recv,
    wring_send, wring_recv, wmate_send, wmate_recv, cross_send, cross_recv,
    fetch, ag_send, ag_recv,
    *scatter_sems,
):
    grp, sp, tp = lax.axis_index("grp"), lax.axis_index("sp"), lax.axis_index("tp")
    count = 2 * chips
    core = lax.rem(sp, 2)
    mate = sp + 1 - 2 * core
    parity = lax.rem(grp, 2)
    twin = grp + 1 - 2 * parity
    above, below = lax.rem(sp + 2, count), lax.rem(sp + count - 2, count)
    right, left, across = lax.rem(tp + 1, 4), lax.rem(tp + 3, 4), lax.rem(tp + 2, 4)
    half = chips // 2
    tokens = nq.shape[0]
    nwidth, wwidth = ngain.shape[1], wgain.shape[1]

    barrier = pltpu.get_barrier_semaphore()
    greeted = ({"sp": above}, {"sp": below}, {"sp": mate}, {"tp": right}, {"tp": left}, {"grp": twin})
    for where in greeted:
        pl.semaphore_signal(barrier, inc=1, device_id=where, device_id_type=MESH)
    nrows = outn.shape[0]
    loads = (
        pltpu.make_async_copy(gate_shard, weights.at[0, sp], fetch.at[0]),
        pltpu.make_async_copy(up_shard, weights.at[1, sp], fetch.at[1]),
        pltpu.make_async_copy(down_shard, weights.at[2, sp], fetch.at[2]),
        pltpu.make_async_copy(outn, projection.at[:nrows], fetch.at[3]),
        pltpu.make_async_copy(outw, projection.at[nrows:], fetch.at[4]),
    )
    for copy in loads:
        copy.start()

    wholes = (gn, gw)

    def ring(piece, way, slot, target):
        whole = wholes[piece]
        return pltpu.make_async_remote_copy(
            whole.at[slot, core],
            whole.at[target, core],
            ring_send.at[piece, way, slot],
            ring_recv.at[piece, target],
            {"sp": above if way == 0 else below},
            MESH,
        )

    def to_mate(piece, slot):
        whole = wholes[piece]
        return pltpu.make_async_remote_copy(
            whole.at[slot, core],
            whole.at[slot, core],
            mate_send.at[piece, slot],
            mate_recv.at[piece, slot],
            {"sp": mate},
            MESH,
        )

    def arrive(piece, slot):
        ring(piece, 0, slot, slot).wait_recv()

    share = (parity, 2, 1 - parity)

    def source(slot):
        back = jnp.where(slot <= half, count - 2 * slot, 2 * (slot - half))
        return lax.rem(sp + back, count)

    def wring(kind, way, slot, target):
        block = weights.at[share[kind], source(slot)]
        return pltpu.make_async_remote_copy(
            block,
            block,
            wring_send.at[kind, way, slot],
            wring_recv.at[kind, target],
            {"sp": above if way == 0 else below},
            MESH,
        )

    def wmate(kind, slot):
        block = weights.at[share[kind], source(slot)]
        return pltpu.make_async_remote_copy(
            block, block, wmate_send.at[kind, slot], wmate_recv.at[kind, slot], {"sp": mate}, MESH
        )

    def cross(slot):
        block = weights.at[share[0], source(slot)]
        return pltpu.make_async_remote_copy(
            block, block, cross_send.at[slot], cross_recv.at[slot], {"grp": twin}, MESH
        )

    def serve_share(step, last=False):
        wring(0, 0, step, step).wait_recv()
        if not last:
            wring(0, 0, step, step + 1).start()
        cross(step).start()
        wmate(0, step).start()
        if last:
            return
        wring(0, 0, half + step, half + step).wait_recv()
        if not (isinstance(step, int) and step + 1 == half):
            wring(0, 1, half + step, half + step + 1).start()
        cross(half + step).start()
        wmate(0, half + step).start()

    def serve_down(step):
        wring(1, 0, step, step).wait_recv()
        if step + 1 < half:
            wring(1, 0, step, step + 1).start()
        wmate(1, step).start()
        if step < half:
            wring(1, 0, half + step, half + step).wait_recv()
            wring(1, 1, half + step, half + step + 1 if step + 1 < half else half).start()
            wmate(1, half + step).start()

    def serve_cross(step):
        cross(step).wait_recv()
        wmate(2, step).start()
        if step < half:
            cross(half + step).wait_recv()
            wmate(2, half + step).start()

    positions = sp * tokens + lax.broadcasted_iota(jnp.int32, (tokens, freqs.shape[1]), 0)
    grid_row = (positions // GRID).astype(F32)
    grid_column = (positions % GRID).astype(F32)
    angles = jnp.where(freqs[1:2, :] > 0.5, grid_row, grid_column) * freqs[0:1, :]
    cosine, sine = jnp.cos(angles), jnp.sin(angles)
    first = 0
    for table, width in ((wtable, wwidth), (ntable, nwidth)):
        c, z = (x[:, first : first + width // 2] for x in (cosine, sine))
        table[...] = jnp.concatenate([c, c, -z, z], axis=1)
        first += width // 2
    gn[0, core] = jnp.concatenate(
        [prepared(nkv[:, :nwidth], ngain[1:2, :], ntable[...]), nkv[:, nwidth:]], axis=1
    )
    gw[0, core, :, :wwidth] = prepared(wkv[:, :wwidth], wgain[1:2, :], wtable[...])
    gw[0, core, :, wwidth:] = wkv[:, wwidth:]
    pl.semaphore_wait(barrier, len(greeted))
    for piece in (0, 1):
        ring(piece, 0, 0, 1).start()
        ring(piece, 1, 0, half + 1).start()
        to_mate(piece, 0).start()
    for copy in loads[:2]:
        copy.wait()
    wring(0, 0, 0, 1).start()
    wring(0, 1, 0, half + 1).start()
    wmate(0, 0).start()
    wmate(2, 0).start()

    zeros = jnp.zeros((tokens, qn.shape[1] - nwidth), BF16)
    for head in range(qn.shape[0] // tokens):
        raw = nq[:, head * nwidth : (head + 1) * nwidth]
        turned = prepared(raw, ngain[0:1, :], ntable[...])
        qn[head * tokens : (head + 1) * tokens, :] = jnp.concatenate([turned, zeros], axis=1)
    for head in range(qw.shape[0] // tokens):
        raw = wq[:, head * wwidth : (head + 1) * wwidth]
        qw[head * tokens : (head + 1) * tokens, :] = prepared(raw, wgain[0:1, :], wtable[...])
    narrow = Group(gn, qn, npeak, nsum, nwidth, 256)
    wide = Group(gw, qw, wpeak, wsum, wwidth, 256)
    narrow.start()
    wide.start()
    groups = (narrow, wide)
    for copy in loads[2:]:
        copy.wait()

    def absorb(piece, *slots):
        for slot in slots:
            to_mate(piece, slot).wait_recv()
        groups[piece].absorb(slots)

    def pass_on(piece, step):
        @pl.when(step < half)
        def _():
            arrive(piece, step)
            if piece == 1:
                ring(piece, 0, step, step + 1).start()
            else:

                @pl.when(step + 1 < half)
                def _():
                    ring(piece, 0, step, step + 1).start()

            to_mate(piece, step).start()
            arrive(piece, half + step)
            if piece == 0:
                ring(piece, 1, half + step, jnp.where(step + 1 < half, half + step + 1, half)).start()
            else:

                @pl.when(step + 1 < half)
                def _():
                    ring(piece, 1, half + step, half + step + 1).start()

            to_mate(piece, half + step).start()

        @pl.when(step == half)
        def _():
            arrive(piece, half)
            to_mate(piece, half).start()

    absorb(0, 0)
    absorb(1, 0)
    early = half // 2

    def turn(step, carry):
        pass_on(0, step)

        @pl.when(step > 1)
        def _():
            absorb(1, step - 1, half + step - 1)

        pass_on(1, step)

        @pl.when(lax.rem(step, 2) == 0)
        def _():
            serve_share(step // 2)

        absorb(0, step, half + step)
        return carry

    lax.fori_loop(1, half, turn, 0)
    pass_on(0, jnp.int32(half))
    absorb(1, half - 1, chips - 1)
    pass_on(1, jnp.int32(half))
    serve_share(early)
    absorb(0, half)

    def begin_down():
        wring(1, 0, 0, 1).start()
        wring(1, 1, 0, half + 1).start()
        wmate(1, 0).start()

    events = [functools.partial(serve_share, early + 1), functools.partial(begin_down)]
    shares = [functools.partial(serve_share, k, k == half) for k in range(early + 2, half + 1)]
    crosses = [functools.partial(serve_cross, k) for k in range(1, half + 1)]
    downs = [functools.partial(serve_down, k) for k in range(1, half + 1)]
    order = "xcxcccxcdcdcddcdcddd"
    lanes = {"x": shares, "c": crosses, "d": downs}
    for letter in order:
        if lanes[letter]:
            events.append(lanes[letter].pop(0))
    for left_over in lanes.values():
        events.extend(left_over)

    def serve():
        if events:
            events.pop(0)()

    absorb(1, half)
    serve()
    serve()

    narrow_rows, wide_rows = narrow.finished(), wide.finished()
    low = 0
    for result, width in ((narrow_rows, nwidth), (wide_rows, wwidth)):
        for head in range(result.shape[0] // tokens):
            attn[:, low : low + width] = result[head * tokens : (head + 1) * tokens]
            low += width

    chunk = part.shape[3]

    def emit(c):
        terms = nn(attn[...], projection[:, c * chunk : (c + 1) * chunk]).astype(BF16)
        part[c] = terms.reshape(part.shape[1:])

    def dest(j):
        return {"tp": j}

    first, second = scatter_sems[:6], scatter_sems[6:]
    sums = reduce_scatter(dest, part.at[0:CHUNKS], relay.at[0], pair.at[0], direct.at[0], first, "tp", emit, serve)
    stream = residual[...].astype(F32) + jnp.concatenate(sums, axis=1).astype(F32)
    scale = lax.rsqrt(jnp.mean(stream * stream, axis=-1, keepdims=True) + EPS)
    normed = (stream * scale * mgain[...]).astype(BF16)
    split = rows.shape[3]
    rows[0, tp] = normed[:, :split]
    rows[1, tp] = normed[:, split:]

    def gather(h, way, owner):
        return pltpu.make_async_remote_copy(
            rows.at[h, owner],
            rows.at[h, owner],
            ag_send.at[h, way, owner],
            ag_recv.at[h, owner],
            {"tp": right if way == 0 else left},
            MESH,
        )

    gather(0, 0, tp).start()
    gather(1, 1, tp).start()
    gather(1, 0, tp).start()
    gather(0, 1, tp).start()
    serve()
    serve()
    gather(0, 0, left).wait_recv()
    gather(0, 0, left).start()
    gather(1, 0, right).wait_recv()
    gather(1, 1, right).start()
    serve()
    serve()
    for h, owner in ((1, left), (0, right), (0, across), (1, across)):
        gather(h, 0, owner).wait_recv()
        serve()

    def settle(kind):
        def one(slot, carry):
            wmate(kind, slot).wait_recv()
            return carry

        lax.fori_loop(0, chips, one, 0)

    keep = [f for f in events if f.func is not serve_down]
    later = [f for f in events if f.func is serve_down]
    events[:] = []
    for event in keep:
        event()
        if later:
            later.pop(0)()
    settle(0)
    settle(2)
    units = hidden.shape[1]
    model = weights.shape[1] * weights.shape[2]
    def visit(i, carry):
        span = pl.ds(pl.multiple_of(i * 128, 128), 128)
        both = [weights[k, :, :, span].reshape(model, 128) for k in (0, 1)]
        both = jnp.concatenate(both, axis=1)
        product = nn(rows[0].reshape(tokens, split), both[:split])
        product += nn(rows[1].reshape(tokens, split), both[split:])
        gate, up = product[:, :128], product[:, 128:]
        hidden[:, span] = (gate / (1.0 + jnp.exp(-gate)) * up).astype(BF16)
        return carry

    lax.fori_loop(0, units // 128, visit, 0)
    for event in later:
        event()
    settle(1)

    def emit_down(c):
        count_here = chunk // weights.shape[2]
        block = weights[2, c * count_here : (c + 1) * count_here].reshape(chunk, units)
        terms = nt(hidden[...], block).astype(BF16)
        part[CHUNKS + c] = terms.reshape(part.shape[1:])

    sums = reduce_scatter(
        dest, part.at[CHUNKS:], relay.at[1], pair.at[1], direct.at[1], second, "tp", emit_down, lambda: None
    )
    out[...] = (stream + jnp.concatenate(sums, axis=1).astype(F32)).astype(BF16)

    for h, way, owner in ((0, 0, tp), (1, 1, tp), (1, 0, tp), (0, 1, tp), (0, 0, left), (1, 1, right)):
        gather(h, way, owner).wait_send()

    def drain(step, carry):
        back = jnp.where(step == 0, 0, half + step)

        @pl.when(step < half)
        def _():
            ring(1, 0, step, step + 1).wait_send()
            ring(0, 1, back, half).wait_send()
            wring(0, 0, step, step + 1).wait_send()
            wring(1, 1, back, half).wait_send()

        @pl.when(step + 1 < half)
        def _():
            ring(0, 0, step, step + 1).wait_send()
            ring(1, 1, back, half).wait_send()
            wring(1, 0, step, step + 1).wait_send()
            wring(0, 1, back, half).wait_send()

        return carry

    lax.fori_loop(0, half + 1, drain, 0)

    def drain_slots(slot, carry):
        for piece in (0, 1):
            to_mate(piece, slot).wait_send()
        for kind in (0, 1, 2):
            wmate(kind, slot).wait_send()

        @pl.when(slot > 0)
        def _():
            cross(slot).wait_send()

        return carry

    lax.fori_loop(0, chips, drain_slots, 0)


def local(
    chips,
    residual_in,
    narrow_query_rows,
    wide_query_rows,
    narrow_key_value,
    wide_key_value,
    narrow_norm_gains,
    wide_norm_gains,
    out_narrow,
    out_wide,
    mixer_gain,
    mixer_gate,
    mixer_up,
    mixer_down,
):
    tokens = narrow_query_rows.shape[0]
    owned, model = residual_in.shape
    owners = tokens // owned
    nkv = narrow_key_value.reshape(tokens, -1)
    wkv = wide_key_value.reshape(tokens, -1)
    nwidth, wwidth = nkv.shape[1] // 2, wkv.shape[1] // 2
    nrows = narrow_query_rows.shape[1] // nwidth * tokens
    wrows = wide_query_rows.shape[1] // wwidth * tokens
    depth, units = mixer_gate.shape
    chunk = model // CHUNKS
    joint = out_narrow.shape[0] + out_wide.shape[0]
    vmem = pl.BlockSpec(memory_space=pltpu.VMEM)
    hbm = pl.BlockSpec(memory_space=pl.ANY)
    VMEM, DMA = pltpu.VMEM, pltpu.SemaphoreType.DMA

    return pl.pallas_call(
        functools.partial(layer_kernel, chips),
        out_shape=jax.ShapeDtypeStruct((owned, model), BF16),
        in_specs=[vmem] * 9 + [hbm] * 5,
        out_specs=vmem,
        scratch_shapes=[
            VMEM((tokens, 2 * nwidth), F32),
            VMEM((tokens, 2 * wwidth), F32),
            VMEM((3, 2 * chips, depth, units), BF16),
            VMEM((chips, 2, tokens, nkv.shape[1]), BF16),
            VMEM((chips, 2, tokens, wkv.shape[1]), BF16),
            VMEM((nrows, nkv.shape[1]), BF16),
            VMEM((wrows, wwidth), BF16),
            VMEM((1, nrows), F32),
            VMEM((1, wrows), F32),
            VMEM((PAD + nwidth, nrows), F32),
            VMEM((PAD + wwidth, wrows), F32),
            VMEM((tokens, joint), BF16),
            VMEM((joint, model), BF16),
            VMEM((2 * CHUNKS, owners, owned, chunk), BF16),
            VMEM((2, CHUNKS, owned, chunk), BF16),
            VMEM((2, CHUNKS, 2, owned, chunk), BF16),
            VMEM((2, CHUNKS, owned, chunk), BF16),
            VMEM((2, owners, owned, model // 2), BF16),
            VMEM((tokens, units), BF16),
            DMA((2, 2, chips)),
            DMA((2, chips)),
            DMA((2, chips)),
            DMA((2, chips)),
            DMA((2, 2, chips)),
            DMA((2, chips)),
            DMA((3, chips)),
            DMA((3, chips)),
            DMA((chips,)),
            DMA((chips,)),
            DMA((5,)),
            DMA((2, 2, owners)),
            DMA((2, owners)),
            *[DMA((CHUNKS,))] * 12,
        ],
        compiler_params=pltpu.CompilerParams(
            collective_id=0, has_side_effects=True, vmem_limit_bytes=60 * 2**20
        ),
        name="layer",
    )(
        narrow_query_rows,
        wide_query_rows,
        nkv,
        wkv,
        narrow_norm_gains,
        wide_norm_gains,
        jnp.asarray(frequencies(wwidth, nwidth)),
        residual_in,
        mixer_gain.reshape(1, -1),
        mixer_down.T,
        out_narrow,
        out_wide,
        mixer_gate,
        mixer_up,
    )


def solution(mesh):
    placed = (
        P(("grp", "sp", "tp"), None),
        P(("grp", "sp"), "tp"),
        P(("grp", "sp"), "tp"),
        P(("grp", "sp"), "tp", None),
        P(("grp", "sp"), "tp", None),
        P(),
        P(),
        P("tp", None),
        P("tp", None),
        P(),
        P("sp", "tp"),
        P("sp", "tp"),
        P("tp", "sp"),
    )
    return jax.shard_map(
        functools.partial(local, mesh.shape["sp"] // 2),
        mesh=mesh,
        in_specs=placed,
        out_specs=P(("grp", "sp", "tp"), None),
        check_vma=False,
    )
```

time: 198 us -> 173 us (0.87)
  waiting for transfers between devices: 22.1 us -> 0 us
  Pallas kernels: 155 us -> 171 us
  between operations: 13.6 us -> 0.01 us
  other arithmetic: 3.58 us -> 0 us
    all_gather x1 -> x0, waiting for transfers between devices: 22 us -> none  [local(): weights = lax.all_gather(shard, 'sp', axis=0, tiled=True)]
    pallas_call x2 -> x1, Pallas kernels: 155 us -> 171 us  [local(): pl.pallas_call(functools.partial(layer_kernel, chips), out_shape=jax.Shap...]
    concatenate x4 -> x0, other arithmetic: 2.47 us -> none  [the longest x1 1.93 us: local(): shard = jnp.concatenate([mixer_gate, mixer_up, mixer_down.T], axis=1)]
  transfers between devices with their start and end apart: 1 -> 0, of which waited for: 1 -> 0; matrix products, arithmetic and copies ran while one was open for 1% -> 0% of each run, Pallas kernels for 68% -> 0%
where the time goes in v2:
time: 173 us; the launch traced here: 172 us
  Pallas kernels  171 us (99%)
    pallas_call x1, Pallas kernels, local(): pl.pallas_call(functools.partial(layer_kernel, chips), out_shape=jax.Shap...  171 us

profile of v2, /device:TPU:33, one launch (start us, length us, event | category | flops | bytes accessed | tf_op | source)
XLA Modules:
  0.0 172.4 jit_solution(8451673635397482486)
XLA Ops:
  0.0 170.7 %layer.1 = bf16[80,2048]{1,0:T(8,128)(2,1)} custom-call(bf16[320,256]{1,0:T(8,128)(2,1)} %nq.1, bf16[320,256]{1,0:T(8,128)(2,1)} %wq.1, bf16[320,128]{1,0:T(8,128)(2,1)} %bitcast.6, bf16[320,256]{1,0:T(8,128)(2,1)} %bitcast.5, f32[2,64]{1,0:T(2,128)} %ngain.1, f32[2,128]{1,0:T(2,128)} %wgain.1, f32[8,128]{1,0:T(8,128)} %constant.2.clone.freqs, ...), custom_call_target="tpu_custom_call" | custom-call | tf_op jit(solution)/shard_map/layer/pallas_call | solution.py:572
  170.7 1.7 copy.16

commit v3 on v2

--- a/solution.py
+++ b/solution.py
@@ -16,6 +16,7 @@
 F32 = jnp.float32
 BF16 = jnp.bfloat16
 CHUNKS = 4
+LATE_CHUNKS = 8
 PAD = 16
 
 
@@ -100,7 +101,8 @@
         return result.T.astype(BF16)
 
 
-def reduce_scatter(dest, part, relay, pair, direct, sems, axis, emit, serve):
+def reduce_scatter(dest, buffers, sems, axis, emit, serve, finish, lag):
+    part, relay, pair, direct = buffers
     send_a, send_b, send_c, recv_a, recv_b, recv_c = sems
     me = lax.axis_index(axis)
     right, left = lax.rem(me + 1, 4), lax.rem(me + 3, 4)
@@ -125,28 +127,32 @@
             pair.at[c, 0], pair.at[c, 1], send_c.at[c], recv_c.at[c], dest(ways(c)[0]), MESH
         )
 
-    for c in range(CHUNKS):
+    def forward(c):
+        relayed(c).wait_recv()
+        ahead, _ = ways(c)
+        pair[c, 0] = (part[c, ahead].astype(F32) + relay[c].astype(F32)).astype(BF16)
+        paired(c).start()
+
+    chunks = part.shape[0]
+    for c in range(chunks):
         emit(c)
         relayed(c).start()
         straight(c).start()
         serve()
-    for c in range(CHUNKS):
-        relayed(c).wait_recv()
-        ahead, _ = ways(c)
-        pair[c, 0] = (part[c, ahead].astype(F32) + relay[c].astype(F32)).astype(BF16)
-        paired(c).start()
+        if c >= lag:
+            forward(c - lag)
+    for c in range(chunks - lag, chunks):
+        forward(c)
         serve()
-    sums = []
-    for c in range(CHUNKS):
+    for c in range(chunks):
         straight(c).wait_recv()
         paired(c).wait_recv()
         total = part[c, me].astype(F32) + direct[c].astype(F32) + pair[c, 1].astype(F32)
-        sums.append(total.astype(BF16))
-    for c in range(CHUNKS):
+        finish(c, total.astype(BF16))
+    for c in range(chunks):
         relayed(c).wait_send()
         straight(c).wait_send()
         paired(c).wait_send()
-    return sums
 
 
 def layer_kernel(
@@ -155,7 +161,7 @@
     outn, outw, gate_shard, up_shard,
     out,
     ntable, wtable, weights, gn, gw, qn, qw, npeak, wpeak, nsum, wsum, attn, projection,
-    part, relay, pair, direct, rows, hidden,
+    part, relay, pair, direct, part2, relay2, pair2, direct2, stream, rows, hidden,
     ring_send, ring_recv, mate_send, mate_recv,
     wring_send, wring_recv, wmate_send, wmate_recv, cross_send, cross_recv,
     fetch, ag_send, ag_recv,
@@ -190,12 +196,15 @@
 
     wholes = (gn, gw)
 
+    def sent(way, slot):
+        return slot if way == 0 else jnp.where(slot == 0, half, slot)
+
     def ring(piece, way, slot, target):
         whole = wholes[piece]
         return pltpu.make_async_remote_copy(
             whole.at[slot, core],
             whole.at[target, core],
-            ring_send.at[piece, way, slot],
+            ring_send.at[piece, sent(way, slot)],
             ring_recv.at[piece, target],
             {"sp": above if way == 0 else below},
             MESH,
@@ -221,17 +230,40 @@
         back = jnp.where(slot <= half, count - 2 * slot, 2 * (slot - half))
         return lax.rem(sp + back, count)
 
-    def wring(kind, way, slot, target):
-        block = weights.at[share[kind], source(slot)]
+    def wring(kind, part, way, slot, target):
+        depth = weights.shape[2] // 2
+        block = weights.at[share[kind], source(slot), pl.ds(part * depth, depth)]
         return pltpu.make_async_remote_copy(
             block,
             block,
-            wring_send.at[kind, way, slot],
-            wring_recv.at[kind, target],
+            wring_send.at[kind, part, sent(way, slot)],
+            wring_recv.at[kind, part, target],
             {"sp": above if way == 0 else below},
             MESH,
         )
 
+    def wsend(kind):
+        for part in (0, 1):
+            wring(kind, part, 0, 0, 1).start()
+            wring(kind, part, 1, 0, half + 1).start()
+        wmate(kind, 0).start()
+
+    def wpass(kind, step):
+        if isinstance(step, int) and step == half:
+            for part in (0, 1):
+                wring(kind, part, 0, step, step).wait_recv()
+            return
+        final = isinstance(step, int) and step + 1 == half
+        for part in (0, 1):
+            wring(kind, part, 0, step, step).wait_recv()
+            if not final or part == 0:
+                wring(kind, part, 0, step, step + 1).start()
+            wring(kind, part, 0, half + step, half + step).wait_recv()
+            if not final:
+                wring(kind, part, 1, half + step, half + step + 1).start()
+            elif part == 1:
+                wring(kind, part, 1, half + step, half).start()
+
     def wmate(kind, slot):
         block = weights.at[share[kind], source(slot)]
         return pltpu.make_async_remote_copy(
@@ -244,29 +276,19 @@
             block, block, cross_send.at[slot], cross_recv.at[slot], {"grp": twin}, MESH
         )
 
-    def serve_share(step, last=False):
-        wring(0, 0, step, step).wait_recv()
-        if not last:
-            wring(0, 0, step, step + 1).start()
-        cross(step).start()
-        wmate(0, step).start()
-        if last:
-            return
-        wring(0, 0, half + step, half + step).wait_recv()
-        if not (isinstance(step, int) and step + 1 == half):
-            wring(0, 1, half + step, half + step + 1).start()
-        cross(half + step).start()
-        wmate(0, half + step).start()
+    def slots_of(step):
+        return (step,) if isinstance(step, int) and step == half else (step, half + step)
+
+    def serve_share(step):
+        wpass(0, step)
+        for slot in slots_of(step):
+            cross(slot).start()
+            wmate(0, slot).start()
 
     def serve_down(step):
-        wring(1, 0, step, step).wait_recv()
-        if step + 1 < half:
-            wring(1, 0, step, step + 1).start()
-        wmate(1, step).start()
-        if step < half:
-            wring(1, 0, half + step, half + step).wait_recv()
-            wring(1, 1, half + step, half + step + 1 if step + 1 < half else half).start()
-            wmate(1, half + step).start()
+        wpass(1, step)
+        for slot in slots_of(step):
+            wmate(1, slot).start()
 
     def serve_cross(step):
         cross(step).wait_recv()
@@ -275,6 +297,11 @@
             cross(half + step).wait_recv()
             wmate(2, half + step).start()
 
+    pl.semaphore_wait(barrier, len(greeted))
+    for copy in loads[:2]:
+        copy.wait()
+    wsend(0)
+    wmate(2, 0).start()
     positions = sp * tokens + lax.broadcasted_iota(jnp.int32, (tokens, freqs.shape[1]), 0)
     grid_row = (positions // GRID).astype(F32)
     grid_column = (positions % GRID).astype(F32)
@@ -290,17 +317,10 @@
     )
     gw[0, core, :, :wwidth] = prepared(wkv[:, :wwidth], wgain[1:2, :], wtable[...])
     gw[0, core, :, wwidth:] = wkv[:, wwidth:]
-    pl.semaphore_wait(barrier, len(greeted))
     for piece in (0, 1):
         ring(piece, 0, 0, 1).start()
         ring(piece, 1, 0, half + 1).start()
         to_mate(piece, 0).start()
-    for copy in loads[:2]:
-        copy.wait()
-    wring(0, 0, 0, 1).start()
-    wring(0, 1, 0, half + 1).start()
-    wmate(0, 0).start()
-    wmate(2, 0).start()
 
     zeros = jnp.zeros((tokens, qn.shape[1] - nwidth), BF16)
     for head in range(qn.shape[0] // tokens):
@@ -377,32 +397,72 @@
     absorb(1, half - 1, chips - 1)
     pass_on(1, jnp.int32(half))
     serve_share(early)
+    wsend(1)
     absorb(0, half)
 
-    def begin_down():
-        wring(1, 0, 0, 1).start()
-        wring(1, 1, 0, half + 1).start()
-        wmate(1, 0).start()
-
-    events = [functools.partial(serve_share, early + 1), functools.partial(begin_down)]
-    shares = [functools.partial(serve_share, k, k == half) for k in range(early + 2, half + 1)]
-    crosses = [functools.partial(serve_cross, k) for k in range(1, half + 1)]
-    downs = [functools.partial(serve_down, k) for k in range(1, half + 1)]
-    order = "xcxcccxcdcdcddcdcddd"
-    lanes = {"x": shares, "c": crosses, "d": downs}
-    for letter in order:
-        if lanes[letter]:
-            events.append(lanes[letter].pop(0))
-    for left_over in lanes.values():
-        events.extend(left_over)
+    def drain_keys():
+        def one(step, carry):
+            back = jnp.where(step == 0, 0, half + step)
+
+            @pl.when(step < half)
+            def _():
+                ring(1, 0, step, step + 1).wait_send()
+                ring(0, 1, back, half).wait_send()
+
+            @pl.when(step + 1 < half)
+            def _():
+                ring(0, 0, step, step + 1).wait_send()
+                ring(1, 1, back, half).wait_send()
+
+            return carry
+
+        def mates(slot, carry):
+            for piece in (0, 1):
+                to_mate(piece, slot).wait_send()
+            return carry
+
+        lax.fori_loop(0, half, one, 0)
+        lax.fori_loop(0, chips, mates, 0)
+
+    def drain_weights(kind):
+        def one(step, carry):
+            back = jnp.where(step == 0, 0, half + step)
+            wring(kind, 0, 0, step, step + 1).wait_send()
+            wring(kind, 1, 1, back, half).wait_send()
+
+            @pl.when(step + 1 < half)
+            def _():
+                wring(kind, 1, 0, step, step + 1).wait_send()
+                wring(kind, 0, 1, back, half).wait_send()
+
+            return carry
+
+        def mates(slot, carry):
+            wmate(kind, slot).wait_send()
+            if kind == 0:
+                wmate(2, slot).wait_send()
+
+                @pl.when(slot > 0)
+                def _():
+                    cross(slot).wait_send()
+
+            return carry
+
+        lax.fori_loop(0, half, one, 0)
+        lax.fori_loop(0, chips, mates, 0)
+
+    kinds = {"x": serve_share, "c": serve_cross, "d": serve_down}
+    plan = ["", "", "", "x5", "", "d1", "", "x6k0", "d2c1c2c3c4", "", "x7c5", "d3", "x8", "c6", "d4c7"]
 
     def serve():
-        if events:
-            events.pop(0)()
+        hook = plan.pop(0)
+        for kind, step in zip(hook[::2], hook[1::2]):
+            if kind == "k":
+                drain_keys()
+            else:
+                kinds[kind](int(step))
 
     absorb(1, half)
-    serve()
-    serve()
 
     narrow_rows, wide_rows = narrow.finished(), wide.finished()
     low = 0
@@ -420,11 +480,22 @@
     def dest(j):
         return {"tp": j}
 
-    first, second = scatter_sems[:6], scatter_sems[6:]
-    sums = reduce_scatter(dest, part.at[0:CHUNKS], relay.at[0], pair.at[0], direct.at[0], first, "tp", emit, serve)
-    stream = residual[...].astype(F32) + jnp.concatenate(sums, axis=1).astype(F32)
-    scale = lax.rsqrt(jnp.mean(stream * stream, axis=-1, keepdims=True) + EPS)
-    normed = (stream * scale * mgain[...]).astype(BF16)
+    sums = {}
+    reduce_scatter(
+        dest,
+        (part, relay, pair, direct),
+        scatter_sems[:6],
+        "tp",
+        emit,
+        serve,
+        sums.__setitem__,
+        CHUNKS,
+    )
+    attended = jnp.concatenate([sums[c] for c in range(CHUNKS)], axis=1)
+    kept = residual[...].astype(F32) + attended.astype(F32)
+    stream[...] = kept
+    scale = lax.rsqrt(jnp.mean(kept * kept, axis=-1, keepdims=True) + EPS)
+    normed = (kept * scale * mgain[...]).astype(BF16)
     split = rows.shape[3]
     rows[0, tp] = normed[:, :split]
     rows[1, tp] = normed[:, split:]
@@ -444,12 +515,11 @@
     gather(1, 0, tp).start()
     gather(0, 1, tp).start()
     serve()
-    serve()
     gather(0, 0, left).wait_recv()
     gather(0, 0, left).start()
+    serve()
     gather(1, 0, right).wait_recv()
     gather(1, 1, right).start()
-    serve()
     serve()
     for h, owner in ((1, left), (0, right), (0, across), (1, across)):
         gather(h, 0, owner).wait_recv()
@@ -462,13 +532,8 @@
 
         lax.fori_loop(0, chips, one, 0)
 
-    keep = [f for f in events if f.func is not serve_down]
-    later = [f for f in events if f.func is serve_down]
-    events[:] = []
-    for event in keep:
-        event()
-        if later:
-            later.pop(0)()
+    serve_cross(half)
+    serve_down(half - 3)
     settle(0)
     settle(2)
     units = hidden.shape[1]
@@ -483,59 +548,67 @@
         hidden[:, span] = (gate / (1.0 + jnp.exp(-gate)) * up).astype(BF16)
         return carry
 
-    lax.fori_loop(0, units // 128, visit, 0)
-    for event in later:
-        event()
-    settle(1)
+    blocks = units // 128
+    early_blocks = 2 * blocks // 3
+    lax.fori_loop(0, early_blocks, visit, 0)
+    serve_down(half - 2)
+    lax.fori_loop(early_blocks, blocks, visit, 0)
+    due = {2: half - 1, 5: half}
+
+    depth = weights.shape[2]
+    arrival = [0]
+    for k in range(1, half):
+        arrival += [k, half + k]
+    arrival.append(half)
+    per = part2.shape[3] // (2 * depth)
+
+    def columns(slot):
+        return pl.ds(pl.multiple_of(depth * (source(slot) - core), 2 * depth), 2 * depth)
 
     def emit_down(c):
-        count_here = chunk // weights.shape[2]
-        block = weights[2, c * count_here : (c + 1) * count_here].reshape(chunk, units)
-        terms = nt(hidden[...], block).astype(BF16)
-        part[CHUNKS + c] = terms.reshape(part.shape[1:])
-
-    sums = reduce_scatter(
-        dest, part.at[CHUNKS:], relay.at[1], pair.at[1], direct.at[1], second, "tp", emit_down, lambda: None
+        mine = arrival[c * per : (c + 1) * per]
+        if c in due:
+            serve_down(due[c])
+        pieces = []
+        for slot in mine:
+            wmate(1, slot).wait_recv()
+            both = weights[2, pl.ds(source(slot) - core, 2)]
+            pieces.append(both.reshape(2 * depth, units))
+        terms = nt(hidden[...], jnp.concatenate(pieces, axis=0)).astype(BF16)
+        part2[c] = terms.reshape(part2.shape[1:])
+
+    def finish_down(c, total):
+        for k, slot in enumerate(arrival[c * per : (c + 1) * per]):
+            span = columns(slot)
+            piece = total[:, k * 2 * depth : (k + 1) * 2 * depth]
+            out[:, span] = (stream[:, span] + piece.astype(F32)).astype(BF16)
+
+    reduce_scatter(
+        dest,
+        (part2, relay2, pair2, direct2),
+        scatter_sems[6:],
+        "tp",
+        emit_down,
+        lambda: None,
+        finish_down,
+        3,
     )
-    out[...] = (stream + jnp.concatenate(sums, axis=1).astype(F32)).astype(BF16)
+    drain_weights(0)
 
     for h, way, owner in ((0, 0, tp), (1, 1, tp), (1, 0, tp), (0, 1, tp), (0, 0, left), (1, 1, right)):
         gather(h, way, owner).wait_send()
 
-    def drain(step, carry):
-        back = jnp.where(step == 0, 0, half + step)
-
-        @pl.when(step < half)
-        def _():
-            ring(1, 0, step, step + 1).wait_send()
-            ring(0, 1, back, half).wait_send()
-            wring(0, 0, step, step + 1).wait_send()
-            wring(1, 1, back, half).wait_send()
-
-        @pl.when(step + 1 < half)
-        def _():
-            ring(0, 0, step, step + 1).wait_send()
-            ring(1, 1, back, half).wait_send()
-            wring(1, 0, step, step + 1).wait_send()
-            wring(0, 1, back, half).wait_send()
-
-        return carry
-
-    lax.fori_loop(0, half + 1, drain, 0)
-
-    def drain_slots(slot, carry):
-        for piece in (0, 1):
-            to_mate(piece, slot).wait_send()
-        for kind in (0, 1, 2):
-            wmate(kind, slot).wait_send()
-
-        @pl.when(slot > 0)
-        def _():
-            cross(slot).wait_send()
-
-        return carry
-
-    lax.fori_loop(0, chips, drain_slots, 0)
+    drain_weights(1)
+
+
+def scatter_scratch(chunks, owners, owned, model):
+    chunk = model // chunks
+    return [
+        pltpu.VMEM((chunks, owners, owned, chunk), BF16),
+        pltpu.VMEM((chunks, owned, chunk), BF16),
+        pltpu.VMEM((chunks, 2, owned, chunk), BF16),
+        pltpu.VMEM((chunks, owned, chunk), BF16),
+    ]
 
 
 def local(
@@ -563,7 +636,6 @@
     nrows = narrow_query_rows.shape[1] // nwidth * tokens
     wrows = wide_query_rows.shape[1] // wwidth * tokens
     depth, units = mixer_gate.shape
-    chunk = model // CHUNKS
     joint = out_narrow.shape[0] + out_wide.shape[0]
     vmem = pl.BlockSpec(memory_space=pltpu.VMEM)
     hbm = pl.BlockSpec(memory_space=pl.ANY)
@@ -588,18 +660,17 @@
             VMEM((PAD + wwidth, wrows), F32),
             VMEM((tokens, joint), BF16),
             VMEM((joint, model), BF16),
-            VMEM((2 * CHUNKS, owners, owned, chunk), BF16),
-            VMEM((2, CHUNKS, owned, chunk), BF16),
-            VMEM((2, CHUNKS, 2, owned, chunk), BF16),
-            VMEM((2, CHUNKS, owned, chunk), BF16),
+            *scatter_scratch(CHUNKS, owners, owned, model),
+            *scatter_scratch(LATE_CHUNKS, owners, owned, model),
+            VMEM((owned, model), F32),
             VMEM((2, owners, owned, model // 2), BF16),
             VMEM((tokens, units), BF16),
-            DMA((2, 2, chips)),
+            DMA((2, chips)),
             DMA((2, chips)),
             DMA((2, chips)),
             DMA((2, chips)),
             DMA((2, 2, chips)),
-            DMA((2, chips)),
+            DMA((2, 2, chips)),
             DMA((3, chips)),
             DMA((3, chips)),
             DMA((chips,)),
@@ -607,7 +678,8 @@
             DMA((5,)),
             DMA((2, 2, owners)),
             DMA((2, owners)),
-            *[DMA((CHUNKS,))] * 12,
+            *[DMA((CHUNKS,))] * 6,
+            *[DMA((LATE_CHUNKS,))] * 6,
         ],
         compiler_params=pltpu.CompilerParams(
             collective_id=0, has_side_effects=True, vmem_limit_bytes=60 * 2**20

time: 173 us -> 151 us (0.87)
  Pallas kernels: 171 us -> 149 us
    pallas_call x1, Pallas kernels: 171 us -> 149 us  [local(): pl.pallas_call(functools.partial(layer_kernel, chips), out_shape=jax.Shap...]
where the time goes in v3:
time: 151 us; the launch traced here: 150 us
  Pallas kernels  149 us (99%)
  local copies, waits for them, and re-layouts  1.72 us (1%)
    pallas_call x1, Pallas kernels, local(): pl.pallas_call(functools.partial(layer_kernel, chips), out_shape=jax.Shap...  149 us

profile of v3, /device:TPU:33, one launch (start us, length us, event | category | flops | bytes accessed | tf_op | source)
XLA Modules:
  0.0 150.3 jit_solution(3440775539287112581)
XLA Ops:
  0.0 148.6 %layer.1 = bf16[80,2048]{1,0:T(8,128)(2,1)} custom-call(bf16[320,256]{1,0:T(8,128)(2,1)} %nq.1, bf16[320,256]{1,0:T(8,128)(2,1)} %wq.1, bf16[320,128]{1,0:T(8,128)(2,1)} %bitcast.6, bf16[320,256]{1,0:T(8,128)(2,1)} %bitcast.5, f32[2,64]{1,0:T(2,128)} %ngain.1, f32[2,128]{1,0:T(2,128)} %wgain.1, f32[8,128]{1,0:T(8,128)} %constant.2.clone.freqs, ...), custom_call_target="tpu_custom_call" | custom-call | tf_op jit(solution)/shard_map/layer/pallas_call | solution.py:644
  148.6 1.7 %copy.16 = bf16[80,2048]{1,0:T(8,128)(2,1)} copy(bf16[80,2048]{1,0:T(8,128)(2,1)} %layer.1) | data formatting | bytes 655360
